TPU v7x, 32 devices: a whole 2x2x4 slice. The times are simulated.
32 devices in a mesh: sp: 4 (over z), fs: 4 (over y, x), tp: 2 (over core).
Axes of the slice: x: 2, y: 2, z: 4, core: 2. Of those that a mesh axis runs over, the one named last changes fastest.
Arguments:
- tokens: bfloat16 [2048, 2048], P(('fs', 'sp')), parts along dimension 0, may hold values from -6 to 6
- norm_gain: bfloat16 [2048], replicated, may hold values from 0.099609375 to 1.8984375
- query_down: bfloat16 [2048, 512], P('sp'), may hold values from -0.125 to 0.125
- query_gain: bfloat16 [512], replicated, may hold values from 0.099609375 to 1.8984375
- latent_down: bfloat16 [2048, 256], replicated, may hold values from -0.125 to 0.125
- latent_gain: bfloat16 [256], replicated, may hold values from 0.099609375 to 1.8984375
- rope_down: bfloat16 [2048, 64], replicated, may hold values from -30 to 30
- query_up: bfloat16 [512, 1536], P(None, 'tp'), may hold values from -0.25 to 0.25
- key_up: bfloat16 [256, 1024], P(None, 'tp'), may hold values from -0.75 to 0.75
- value_up: bfloat16 [256, 1024], P(None, 'tp'), may hold values from -0.375 to 0.375
- glu_value: bfloat16 [2048, 1024], P('sp', 'tp'), may hold values from -0.125 to 0.125
- glu_gate: bfloat16 [2048, 1024], P('sp', 'tp'), may hold values from -0.125 to 0.125
- conv_taps: bfloat16 [31, 1024], P(None, 'tp'), may hold values from -1 to 1
- group_gain: bfloat16 [1024], P('tp'), may hold values from 0.099609375 to 1.8984375
- head_proj: bfloat16 [1024, 2048], P('tp', 'sp'), may hold values from -0.75 to 0.75
- channel_proj: bfloat16 [1024, 2048], P('tp', 'sp'), may hold values from -0.1875 to 0.1875
Outputs:
- mixed_out: bfloat16 [2048, 2048], P(('fs', 'sp'), 'tp'), parts along dimension 0
- log_weight: float32 [8, 2048], P('tp', ('fs', 'sp')), parts along dimension 1
There are 4 independent parts, one for each index of `fs`. A program takes and returns all parts, laid end to end along the dimension named above; an argument that names none is the same for every part. Nothing has to cross between parts.
All inputs are finite; a program needn't handle non-finite values.
Results may differ from a plain program's by a relative error of at most 0.015.
The roundings to bfloat16 on the way count: a program that leaves them out, or rounds other values in their place, can miss the bound.
Values may be sent and summed in bfloat16 or wider, within the bound.
A program may use at most 128 MiB of HBM per device.

v0:
```python
import functools

import jax
import jax.numpy as jnp
import numpy as np
from jax import lax
from jax.experimental import pallas as pl
from jax.experimental.pallas import tpu as pltpu
from jax.sharding import PartitionSpec as P

NOPE = 128
ROPE = 64
VDIM = 128
KVR = 256
CH = 1024
GROUPS = 8
GRID_W = 64


norm_eps = 1e-06
rope_base = 10000.0
far_below = -1e30


def padded_2(block, sides, width):
    for axis, dim in sides:
        count = lax.axis_size(axis)
        forward = [(i, i + 1) for i in range(count - 1)]
        backward = [(target, source) for source, target in forward]
        low = lax.ppermute(
            lax.slice_in_dim(block, block.shape[dim] - width, None, axis=dim), axis, forward
        )
        high = lax.ppermute(lax.slice_in_dim(block, 0, width, axis=dim), axis, backward)
        block = jnp.concatenate([low, block, high], axis=dim)
    return block


def rms_scale(values, scale_gain):
    inv_rms = lax.rsqrt(jnp.mean(values * values, axis=-1, keepdims=True) + norm_eps)
    return values * inv_rms * scale_gain.astype(jnp.float32)


def angles_for(positions, rope_size):
    quarter = rope_size // 4
    inverse = rope_base ** (-jnp.arange(quarter, dtype=jnp.float32) / quarter)
    grid_row = (positions // GRID_W).astype(jnp.float32)
    grid_col = (positions % GRID_W).astype(jnp.float32)
    return jnp.concatenate([grid_row[:, None] * inverse, grid_col[:, None] * inverse], axis=-1)


def rotate(values, angles):
    half_size = values.shape[-1] // 2
    front_half = values[..., :half_size]
    back_half = values[..., half_size:]
    cosine = jnp.cos(angles)
    sine_part = jnp.sin(angles)
    return jnp.concatenate(
        [front_half * cosine - back_half * sine_part, back_half * cosine + front_half * sine_part],
        axis=-1,
    )


def key_block(normed, latent_down, latent_gain, rope_down, positions):
    latent = jnp.dot(normed, latent_down, preferred_element_type=jnp.float32)
    latent = rms_scale(latent, latent_gain).astype(jnp.bfloat16)
    rope_key = jnp.dot(normed, rope_down, preferred_element_type=jnp.float32)
    rope_key = rotate(rope_key, angles_for(positions, rope_key.shape[-1])).astype(jnp.bfloat16)
    return jnp.concatenate([latent, rope_key], axis=1)


def per_device(
    tokens,
    norm_gain,
    query_down,
    query_gain,
    latent_down,
    latent_gain,
    rope_down,
    query_up,
    key_up,
    value_up,
    glu_value,
    glu_gate,
    conv_taps,
    group_gain,
    head_proj,
    channel_proj,
):
    tok_count = tokens.shape[0]
    reach_rows = conv_taps.shape[0] // 2
    head_count = key_up.shape[1] // NOPE
    normed = rms_scale(tokens.astype(jnp.float32), norm_gain).astype(jnp.bfloat16)
    offsets = lax.axis_index("sp") * tok_count + jnp.arange(tok_count, dtype=jnp.int32)
    query_latent = jnp.dot(
        normed,
        lax.all_gather(query_down, "sp", axis=0, tiled=True),
        preferred_element_type=jnp.float32,
    )
    value_in = jnp.dot(
        normed,
        lax.all_gather(glu_value, "sp", axis=0, tiled=True),
        preferred_element_type=jnp.float32,
    )
    gate_in = jnp.dot(
        normed,
        lax.all_gather(glu_gate, "sp", axis=0, tiled=True),
        preferred_element_type=jnp.float32,
    )
    latent_query = rms_scale(query_latent, query_gain).astype(jnp.bfloat16)
    query_all = jnp.dot(latent_query, query_up, preferred_element_type=jnp.float32).reshape(
        tok_count, head_count, NOPE + ROPE
    )
    query_plain = query_all[:, :, :NOPE].astype(jnp.bfloat16)
    query_rope = rotate(query_all[:, :, NOPE:], angles_for(offsets, ROPE)[:, None, :]).astype(
        jnp.bfloat16
    )
    absorbed = jnp.einsum(
        "thd,rhd->htr",
        query_plain,
        key_up.reshape(KVR, head_count, NOPE),
        preferred_element_type=jnp.float32,
    ).astype(jnp.bfloat16)
    queries = jnp.concatenate([absorbed, jnp.transpose(query_rope, (1, 0, 2))], axis=-1)
    score_scale = (NOPE + ROPE) ** (-0.5)
    half_rows = tok_count // lax.axis_size("tp")
    first_row = lax.axis_index("tp") * half_rows
    own_rows = lax.dynamic_slice_in_dim(normed, first_row, half_rows, 0)
    own_positions = lax.dynamic_slice_in_dim(offsets, first_row, half_rows, 0)
    own_keys = key_block(own_rows, latent_down, latent_gain, rope_down, own_positions)
    block_keys = lax.all_gather(own_keys, ("sp", "tp"), axis=0, tiled=True)
    row_max = jnp.full((head_count, tok_count), far_below, jnp.float32)
    scores = (
        jnp.einsum("hqc,kc->hqk", queries, block_keys, preferred_element_type=jnp.float32)
        * score_scale
    )
    new_max = jnp.maximum(row_max, jnp.max(scores, axis=2))
    weights = jnp.exp(scores - new_max[:, :, None])
    new_sum = jnp.sum(weights, axis=2)
    added = jnp.einsum(
        "hqk,kr->hqr",
        weights.astype(jnp.bfloat16),
        block_keys[:, :KVR],
        preferred_element_type=jnp.float32,
    )
    gated_rows = (value_in * jax.nn.sigmoid(gate_in)).astype(jnp.bfloat16)
    padded = padded_2(gated_rows, (("sp", 0),), reach_rows)
    filtered = padded[0:tok_count].astype(jnp.float32) * conv_taps[0].astype(jnp.float32)
    for tap_index in range(1, conv_taps.shape[0]):
        filtered = filtered + padded[tap_index : tap_index + tok_count].astype(
            jnp.float32
        ) * conv_taps[tap_index].astype(jnp.float32)
    grouped = filtered.reshape(tok_count, -1, CH // GROUPS)
    centred = grouped - jnp.mean(grouped, axis=-1, keepdims=True)
    spread = jnp.mean(centred * centred, axis=-1, keepdims=True)
    normal_groups = (centred * lax.rsqrt(spread + norm_eps)).reshape(tok_count, -1)
    conv_branch = jax.nn.silu(normal_groups * group_gain.astype(jnp.float32)).astype(jnp.bfloat16)
    attended = (added / new_sum[:, :, None]).astype(jnp.bfloat16)
    log_weight = new_max + jnp.log(new_sum)
    head_out = jnp.einsum(
        "htr,rhv->thv",
        attended,
        value_up.reshape(KVR, head_count, VDIM),
        preferred_element_type=jnp.float32,
    )
    head_out = head_out.reshape(tok_count, head_count * VDIM).astype(jnp.bfloat16)
    mixed_in = jnp.concatenate([head_out, conv_branch], axis=1)
    out_weight = jnp.concatenate([head_proj, channel_proj], axis=0)
    partial_terms = jnp.dot(
        mixed_in,
        lax.all_gather(out_weight, "sp", axis=1, tiled=True),
        preferred_element_type=jnp.float32,
    )
    mixed_out = lax.psum_scatter(
        partial_terms.astype(jnp.bfloat16), "tp", scatter_dimension=1, tiled=True
    )
    return (mixed_out, log_weight)


LANES = 128
MESH = pl.DeviceIdType.MESH
F32 = jnp.float32
BF16 = jnp.bfloat16
Z_IN, X_IN, Y_IN, DX_IN, DY_IN = range(5)
Z_LOW, Z_HIGH, Z_FWD, X_OUT, Y_OUT, DX_OUT, DY_OUT = range(7)


def rope_tables(length):
    quarter = ROPE // 4
    inverse = np.float32(rope_base) ** (-np.arange(quarter, dtype=np.float32) / np.float32(quarter))
    positions = np.arange(length)
    row = (positions // GRID_W).astype(np.float32)[:, None] * inverse
    col = (positions % GRID_W).astype(np.float32)[:, None] * inverse
    angles = np.concatenate([row, col], axis=1).astype(np.float32)
    cosine, sine = np.cos(angles), np.sin(angles)
    tables = np.zeros((3, length, LANES), np.float32)
    half = ROPE // 2
    tables[0, :, :half] = cosine
    tables[0, :, half:ROPE] = cosine
    tables[1, :, :half] = -sine
    tables[2, :, half:ROPE] = sine
    return tables


def dot(a, b):
    return jnp.dot(a, b, preferred_element_type=F32)


def row_of(ref):
    return ref[...].reshape(1, -1)


def dot_nt(a, b):
    return lax.dot_general(a, b, (((1,), (1,)), ((), ())), preferred_element_type=F32)


def fused_kernel(
    n_sp,
    tokens, norm_gain, query_down, query_gain, latent_down, latent_gain, rope_down, query_up,
    key_up, value_up, glu_value, glu_gate, conv_taps, group_gain, head_proj, channel_proj, tables,
    out, log_out,
    w_q, w_v, w_t, w_o, tok_v, lat_v, rope_v, qup_v, kup_v, vup_v, tab_v,
    normed, keys, key_tmp, q_acc, q_lat, q_scr, v_acc, t_acc, mixed, gated, low_rows, high_rows, padded,
    parts, peer_parts,
    load_sem, recv_sem, send_sem, key_recv, key_send, key_pair_recv, key_pair_send, pair_recv, pair_send, halo_recv, halo_send,
):
    z = lax.axis_index("sp")
    c = lax.axis_index("fs")
    t = lax.axis_index("tp")
    peer = 1 - t
    c_x = c + 1 - 2 * (c % 2)
    c_y = (c + 2) % 4
    c_d = 3 - c
    rows = tokens.shape[0]
    depth = query_down.shape[0]
    q_cols = w_q.shape[2]
    chans = glu_value.shape[1]
    heads = key_up.shape[1] // NOPE
    head_rows = head_proj.shape[0]
    out_rows = w_o.shape[1]

    loads = {}

    def load(name, src, dst):
        copy = pltpu.make_async_copy(src, dst, load_sem.at[len(loads)])
        copy.start()
        loads[name] = copy

    load("wq", query_down.at[:, pl.ds(pl.multiple_of(t * q_cols, LANES), q_cols)], w_q.at[z])
    load("gv", glu_value, w_v.at[z])
    load("gg", glu_gate, w_t.at[z])
    load("tok", tokens, tok_v)
    load("lat", latent_down, lat_v)
    load("rope", rope_down, rope_v)
    load("tab", tables.at[:, pl.ds(pl.multiple_of(z * rows, LANES), rows), :], tab_v)
    load("hp", head_proj, w_o.at[z, pl.ds(0, head_rows), :])
    load("cp", channel_proj, w_o.at[z, pl.ds(head_rows, out_rows - head_rows), :])
    load("qup", query_up, qup_v)
    load("kup", key_up, kup_v)
    load("vup", value_up, vup_v)

    barrier = pltpu.get_barrier_semaphore()
    sides = [{"fs": c_x}, {"fs": c_y}, {"tp": peer}]
    for partner in sides:
        pl.semaphore_signal(barrier, inc=1, device_id=partner, device_id_type=MESH)

    @pl.when(z > 0)
    def _():
        pl.semaphore_signal(barrier, inc=1, device_id={"sp": z - 1}, device_id_type=MESH)

    @pl.when(z < n_sp - 1)
    def _():
        pl.semaphore_signal(barrier, inc=1, device_id={"sp": z + 1}, device_id_type=MESH)

    ends = (z == 0).astype(jnp.int32) + (z == n_sp - 1).astype(jnp.int32)
    pl.semaphore_wait(barrier, len(sides) + 2 - ends)

    direct_rows = (out_rows // 8) // 64 * 64
    units = [
        (w_q, 0, depth, True),
        (w_v, 0, depth, True),
        (w_t, 0, depth, True),
        (w_o, 0, head_rows, True),
        (w_o, head_rows, out_rows - head_rows - direct_rows, True),
        (w_o, out_rows - direct_rows, direct_rows, False),
    ]
    Q, V, T, H, P, D = range(6)

    def block(u, shard, quarter, half=None):
        buf, first, count, shared = units[u]
        if not shared:
            return buf.at[shard, pl.ds(first, count), :]
        size = count // 4
        start = first + quarter * size
        if half is not None:
            size = size // 2
            start = start + half * size
        return buf.at[shard, pl.ds(pl.multiple_of(start, 16), size), :]

    def remote(u, shard, ref, out_kind, in_kind, device):
        return pltpu.make_async_remote_copy(
            src_ref=ref, dst_ref=ref,
            send_sem=send_sem.at[u, shard, out_kind], recv_sem=recv_sem.at[u, shard, in_kind],
            device_id=device, device_id_type=MESH,
        )

    def own_copy(u, low):
        return remote(
            u, z, block(u, z, c), Z_LOW if low else Z_HIGH, Z_IN, {"sp": z - 1 if low else z + 1}
        )

    def send_own(u):
        @pl.when(z > 0)
        def _():
            own_copy(u, True).start()

        @pl.when(z < n_sp - 1)
        def _():
            own_copy(u, False).start()

    nearest = jnp.minimum(z, n_sp - 1 - z)
    arrivals = []
    for k in range(n_sp - 1):
        both = k < 2 * nearest
        distance = jnp.where(both, k // 2 + 1, k - nearest + 1)
        from_low = jnp.where(both, 1 - k % 2, (2 * z > n_sp - 1).astype(jnp.int32))
        shard = z - distance * (2 * from_low - 1)
        arrivals.append((shard, z + 2 * from_low - 1))

    def forward_copy(u, k):
        shard, target = arrivals[k]
        return remote(u, shard, block(u, shard, c), Z_FWD, Z_IN, {"sp": target})

    def when_forward(k, action):
        target = arrivals[k][1]

        @pl.when((target >= 0) & (target < n_sp))
        def _():
            action()

    def side_copies(u, k):
        shard, _ = arrivals[k]
        mine = block(u, shard, c)
        return (
            remote(u, shard, mine, X_OUT, X_IN, {"fs": c_x}),
            remote(u, shard, mine, Y_OUT, Y_IN, {"fs": c_y}),
        )

    def corner_copies(u, k):
        shard, _ = arrivals[k]
        return (
            remote(u, shard, block(u, shard, c_x, 0), DY_OUT, DY_IN, {"fs": c_y}),
            remote(u, shard, block(u, shard, c_y, 1), DX_OUT, DX_IN, {"fs": c_x}),
        )

    def wait_in(u, k, kind, quarter, half=None):
        shard, _ = arrivals[k]
        remote(u, shard, block(u, shard, quarter, half), Z_FWD, kind, {"fs": c_x}).wait_recv()

    def step_a(u, k):
        wait_in(u, k, Z_IN, c)
        when_forward(k, lambda: forward_copy(u, k).start())
        if units[u][3]:
            for copy in side_copies(u, k):
                copy.start()

    def step_b(u, k):
        to_y, to_x = corner_copies(u, k)
        wait_in(u, k, X_IN, c_x)
        to_y.start()
        wait_in(u, k, Y_IN, c_y)
        to_x.start()

    def step_c(u, k):
        wait_in(u, k, DY_IN, c_d, 0)
        wait_in(u, k, DX_IN, c_d, 1)

    for name, u in (("wq", Q), ("gv", V), ("gg", T)):
        loads[name].wait()
        send_own(u)

    loads["tok"].wait()
    values = tok_v[...].astype(F32)
    normed[...] = rms_scale(values, row_of(norm_gain)).astype(BF16)

    def rotate_lanes(v):
        half = ROPE // 2
        return (
            v * tab_v[0] + pltpu.roll(v, LANES - half, 1) * tab_v[1] + pltpu.roll(v, half, 1) * tab_v[2]
        )

    loads["lat"].wait()
    latent = rms_scale(dot(normed[...], lat_v[...]), row_of(latent_gain))
    keys[z, :, 0:KVR] = latent.astype(BF16)
    loads["rope"].wait()
    loads["tab"].wait()
    key_tmp[...] = jnp.zeros_like(key_tmp)
    key_tmp[:, 0:ROPE] = dot_nt(normed[...], rope_v[...])
    keys[z, :, KVR : KVR + LANES] = rotate_lanes(key_tmp[...]).astype(BF16)

    half_rows = rows // 2

    def key_half(shard, half):
        return keys.at[shard, pl.ds(pl.multiple_of(half * half_rows, 16), half_rows), :]

    def key_copy(shard, kind, target):
        return pltpu.make_async_remote_copy(
            src_ref=key_half(shard, t), dst_ref=key_half(shard, t),
            send_sem=key_send.at[shard, kind], recv_sem=key_recv.at[shard],
            device_id={"sp": target}, device_id_type=MESH,
        )

    def key_pair(shard, half):
        return pltpu.make_async_remote_copy(
            src_ref=key_half(shard, half), dst_ref=key_half(shard, half),
            send_sem=key_pair_send.at[shard], recv_sem=key_pair_recv.at[shard],
            device_id={"tp": peer}, device_id_type=MESH,
        )

    def own_keys(action):
        @pl.when(z > 0)
        def _():
            action(key_copy(z, Z_LOW, z - 1))

        @pl.when(z < n_sp - 1)
        def _():
            action(key_copy(z, Z_HIGH, z + 1))

    own_keys(lambda copy: copy.start())

    def step_k(k):
        shard, target = arrivals[k]
        key_copy(shard, Z_FWD, target).wait_recv()
        when_forward(k, lambda: key_copy(shard, Z_FWD, target).start())
        key_pair(shard, t).start()

    def add_shard(acc, weights, shard, first=False):
        columns = pl.ds(pl.multiple_of(shard * depth, LANES), depth)
        term = dot(normed[:, columns], weights[shard])
        acc[...] = term if first else acc[...] + term

    add_shard(q_acc, w_q, z, True)
    add_shard(v_acc, w_v, z, True)
    add_shard(t_acc, w_t, z, True)
    accs = {Q: (q_acc, w_q), V: (v_acc, w_v), T: (t_acc, w_t)}

    def step_cm(u, k):
        step_c(u, k)
        add_shard(*accs[u], arrivals[k][0])

    last = n_sp - 2
    loads["hp"].wait()
    loads["cp"].wait()
    for k in range(last + 1):
        for u in (Q, V, T):
            step_a(u, k)
            if k:
                step_b(u, k - 1)
            if k > 1:
                step_cm(u, k - 2)
        step_k(k)
        if k == 1:
            send_own(H)
    send_own(P)
    step_b(Q, last)
    step_a(H, 0)
    step_b(V, last)
    step_a(H, 1)
    step_b(T, last)
    send_own(D)
    for u in (Q, V, T):
        step_cm(u, last - 1)
    step_b(H, 0)
    step_a(P, 0)
    step_cm(Q, last)
    step_a(H, 2)

    q_lat[t] = q_acc[...]
    q_copy = pltpu.make_async_remote_copy(
        src_ref=q_lat.at[t], dst_ref=q_lat.at[t], send_sem=pair_send.at[0], recv_sem=pair_recv.at[0],
        device_id={"tp": peer}, device_id_type=MESH,
    )
    q_copy.start()
    loads["qup"].wait()
    loads["kup"].wait()
    loads["vup"].wait()
    pltpu.make_async_remote_copy(
        src_ref=q_lat.at[peer], dst_ref=q_lat.at[peer], send_sem=pair_send.at[0],
        recv_sem=pair_recv.at[0], device_id={"tp": peer}, device_id_type=MESH,
    ).wait_recv()
    whole_q = jnp.concatenate([q_lat[0], q_lat[1]], axis=1)
    latent_query = rms_scale(whole_q, row_of(query_gain)).astype(BF16)
    q_scr[...] = dot(latent_query, qup_v[...])
    for k in range(n_sp - 1):
        key_pair(arrivals[k][0], peer).wait_recv()

    def attend(h, shifted):
        start = h * (NOPE + ROPE)
        source = q_scr[...]
        if start % LANES:
            source, start = shifted, start - ROPE
        plain = source[:, start : start + NOPE].astype(BF16)
        rope_part = rotate_lanes(source[:, start + NOPE : start + NOPE + LANES]).astype(BF16)
        absorbed = dot_nt(plain, kup_v[:, h * NOPE : (h + 1) * NOPE]).astype(BF16)
        query = jnp.concatenate([absorbed, rope_part], axis=1)
        all_keys = keys[...].reshape(n_sp * rows, KVR + LANES)
        scores = dot_nt(query, all_keys) * (NOPE + ROPE) ** (-0.5)
        row_max = jnp.max(scores, axis=1, keepdims=True)
        weights = jnp.exp(scores - row_max)
        total = jnp.sum(weights, axis=1, keepdims=True)
        added = dot(weights.astype(BF16), all_keys[:, 0:KVR])
        attended = (added / total).astype(BF16)
        head_out = dot(attended, vup_v[:, h * VDIM : (h + 1) * VDIM])
        mixed[:, h * VDIM : (h + 1) * VDIM] = head_out.astype(BF16)
        return row_max + jnp.log(total)

    whole = q_scr[...]
    shifted = pltpu.roll(whole, whole.shape[1] - ROPE, 1)
    lane = lax.broadcasted_iota(jnp.int32, (rows, LANES), 1)
    logs = jnp.zeros((rows, LANES), F32)
    relays = [
        lambda: step_a(P, 1), lambda: step_b(H, 1), lambda: (step_a(D, 0), step_a(P, 2)),
        lambda: step_b(P, 0),
    ]
    for h in range(heads):
        logs = jnp.where(lane == h, attend(h, shifted), logs)
        relays[h]()
    log_out[...] = jnp.transpose(logs)[0:heads, :]

    step_cm(V, last)
    step_cm(T, last)

    halo = low_rows.shape[0]
    reach = conv_taps.shape[0] // 2
    gated[...] = (v_acc[...] * jax.nn.sigmoid(t_acc[...])).astype(BF16)
    up_copy = pltpu.make_async_remote_copy(
        src_ref=gated.at[pl.ds(rows - halo, halo), :], dst_ref=low_rows,
        send_sem=halo_send.at[0], recv_sem=halo_recv.at[0],
        device_id={"sp": z + 1}, device_id_type=MESH,
    )
    down_copy = pltpu.make_async_remote_copy(
        src_ref=gated.at[pl.ds(0, halo), :], dst_ref=high_rows,
        send_sem=halo_send.at[1], recv_sem=halo_recv.at[1],
        device_id={"sp": z - 1}, device_id_type=MESH,
    )

    @pl.when(z < n_sp - 1)
    def _():
        up_copy.start()

    @pl.when(z > 0)
    def _():
        down_copy.start()

    padded[halo : halo + rows, :] = gated[...].astype(F32)
    step_a(D, 1)
    step_b(H, 2)

    @pl.when(z > 0)
    def _():
        up_copy.wait_recv()
        padded[0:halo, :] = low_rows[...].astype(F32)

    @pl.when(z == 0)
    def _():
        padded[0:halo, :] = jnp.zeros((halo, chans), F32)

    @pl.when(z < n_sp - 1)
    def _():
        down_copy.wait_recv()
        padded[halo + rows : 2 * halo + rows, :] = high_rows[...].astype(F32)

    @pl.when(z == n_sp - 1)
    def _():
        padded[halo + rows : 2 * halo + rows, :] = jnp.zeros((halo, chans), F32)

    group = CH // GROUPS
    gains = row_of(group_gain).astype(F32)
    between = [
        lambda: step_b(P, 1), lambda: step_c(H, 0), lambda: step_a(D, 2), lambda: step_b(P, 2),
    ]
    for g in range(chans // group):
        lanes = slice(g * group, (g + 1) * group)
        taps = conv_taps[:, lanes].astype(F32)
        filtered = jnp.zeros((rows, group), F32)
        for j in range(conv_taps.shape[0]):
            first = halo - reach + j
            filtered = filtered + padded[first : first + rows, lanes] * taps[j : j + 1, :]
        centred = filtered - jnp.mean(filtered, axis=1, keepdims=True)
        spread = jnp.mean(centred * centred, axis=1, keepdims=True)
        branch = centred * lax.rsqrt(spread + norm_eps) * gains[:, lanes]
        branch = branch * jax.nn.sigmoid(branch)
        mixed[:, heads * VDIM + g * group : heads * VDIM + (g + 1) * group] = branch.astype(BF16)
        between[g]()

    half_sp = n_sp // 2

    def p_copy(i):
        return pltpu.make_async_remote_copy(
            src_ref=parts.at[peer * half_sp + i], dst_ref=peer_parts.at[i],
            send_sem=pair_send.at[1 + i], recv_sem=pair_recv.at[1 + i],
            device_id={"tp": peer}, device_id_type=MESH,
        )

    def add_part(shard, between_halves):
        part = dot(mixed[:, 0:head_rows], w_o[shard, 0:head_rows, :])
        between_halves()
        part = part + dot(mixed[:, head_rows:out_rows], w_o[shard, head_rows:out_rows, :])
        parts[shard] = part.astype(BF16)
        for i in range(half_sp):
            @pl.when(shard == peer * half_sp + i)
            def _():
                p_copy(i).start()

    add_part(z, lambda: None)
    for k in range(n_sp - 1):
        if k:
            step_c(H, k)
        add_part(arrivals[k][0], functools.partial(step_c, P, k))

    for u in range(len(units)):
        @pl.when(z > 0)
        def _():
            own_copy(u, True).wait_send()

        @pl.when(z < n_sp - 1)
        def _():
            own_copy(u, False).wait_send()

        for k in range(n_sp - 1):
            when_forward(k, lambda: forward_copy(u, k).wait_send())
            if units[u][3]:
                for copy in side_copies(u, k) + corner_copies(u, k):
                    copy.wait_send()
    own_keys(lambda copy: copy.wait_send())
    for k in range(n_sp - 1):
        shard, target = arrivals[k]
        when_forward(k, lambda: key_copy(shard, Z_FWD, target).wait_send())
        key_pair(shard, t).wait_send()
    q_copy.wait_send()

    @pl.when(z < n_sp - 1)
    def _():
        up_copy.wait_send()

    @pl.when(z > 0)
    def _():
        down_copy.wait_send()

    for i in range(half_sp):
        p_copy(i).wait()
    width = parts.shape[2]
    for i in range(half_sp):
        total = parts[t * half_sp + i].astype(F32) + peer_parts[i].astype(F32)
        out[:, i * width : (i + 1) * width] = total.astype(BF16)


def fused_device(n_sp, *args):
    (tokens, norm_gain, query_down, query_gain, latent_down, latent_gain, rope_down, query_up,
     key_up, value_up, glu_value, glu_gate, conv_taps, group_gain, head_proj, channel_proj) = args
    rows, width = tokens.shape
    depth, q_rank = query_down.shape
    chans = glu_value.shape[1]
    heads = key_up.shape[1] // NOPE
    out_rows = head_proj.shape[0] + channel_proj.shape[0]
    cols = head_proj.shape[1]
    halo = (conv_taps.shape[0] // 2 + 15) // 16 * 16
    tables = jnp.asarray(rope_tables(n_sp * rows))
    vmem = pl.BlockSpec(memory_space=pltpu.VMEM)
    hbm = pl.BlockSpec(memory_space=pltpu.HBM)
    as_row = lambda v: v
    operands = [
        (tokens, hbm), (as_row(norm_gain), vmem), (query_down, hbm), (as_row(query_gain), vmem),
        (latent_down, hbm), (as_row(latent_gain), vmem), (rope_down.T, hbm), (query_up, hbm),
        (key_up, hbm), (value_up, hbm), (glu_value, hbm), (glu_gate, hbm), (conv_taps, vmem),
        (as_row(group_gain), vmem), (head_proj, hbm), (channel_proj, hbm), (tables, hbm),
    ]
    like = lambda a: pltpu.VMEM(a.shape, a.dtype)
    dma = pltpu.SemaphoreType.DMA
    scratch = [
        pltpu.VMEM((n_sp, depth, q_rank // 2), BF16),
        pltpu.VMEM((n_sp, depth, chans), BF16),
        pltpu.VMEM((n_sp, depth, chans), BF16),
        pltpu.VMEM((n_sp, out_rows, cols), BF16),
        like(tokens), like(latent_down), pltpu.VMEM(rope_down.shape[::-1], BF16), like(query_up), like(key_up), like(value_up),
        pltpu.VMEM((3, rows, LANES), F32),
        pltpu.VMEM((rows, width), BF16),
        pltpu.VMEM((n_sp, rows, KVR + LANES), BF16),
        pltpu.VMEM((rows, LANES), F32),
        pltpu.VMEM((rows, q_rank // 2), F32),
        pltpu.VMEM((2, rows, q_rank // 2), F32),
        pltpu.VMEM((rows, query_up.shape[1]), F32),
        pltpu.VMEM((rows, chans), F32),
        pltpu.VMEM((rows, chans), F32),
        pltpu.VMEM((rows, out_rows), BF16),
        pltpu.VMEM((rows, chans), BF16),
        pltpu.VMEM((halo, chans), BF16),
        pltpu.VMEM((halo, chans), BF16),
        pltpu.VMEM((rows + 2 * halo, chans), F32),
        pltpu.VMEM((n_sp, rows, cols), BF16),
        pltpu.VMEM((n_sp // 2, rows, cols), BF16),
        dma((12,)), dma((6, n_sp, 5)), dma((6, n_sp, 7)), dma((n_sp,)), dma((n_sp, 3)), dma((n_sp,)),
        dma((n_sp,)),
        dma((1 + n_sp // 2,)), dma((1 + n_sp // 2,)), dma((2,)), dma((2,)),
    ]
    return pl.pallas_call(
        functools.partial(fused_kernel, n_sp),
        out_shape=(
            jax.ShapeDtypeStruct((rows, n_sp * cols // 2), BF16),
            jax.ShapeDtypeStruct((heads, rows), F32),
        ),
        in_specs=[spec for _, spec in operands],
        out_specs=(vmem, vmem),
        scratch_shapes=scratch,
        compiler_params=pltpu.CompilerParams(
            collective_id=0, has_side_effects=True, vmem_limit_bytes=63 * 1024 * 1024
        ),
        name="fused_layer",
    )(*[value for value, _ in operands])


def solution(mesh):
    in_specs = (
        P(("fs", "sp"), None),
        P(),
        P("sp", None),
        P(),
        P(),
        P(),
        P(),
        P(None, "tp"),
        P(None, "tp"),
        P(None, "tp"),
        P("sp", "tp"),
        P("sp", "tp"),
        P(None, "tp"),
        P("tp"),
        P("tp", "sp"),
        P("tp", "sp"),
    )
    out_specs = (P(("fs", "sp"), "tp"), P("tp", ("fs", "sp")))
    body = per_device
    if mesh.shape["fs"] == 4 and mesh.shape["tp"] == 2 and mesh.shape["sp"] == 4:
        body = functools.partial(fused_device, mesh.shape["sp"])
    return jax.shard_map(
        body, mesh=mesh, in_specs=in_specs, out_specs=out_specs, check_vma=False
    )
```

profile of v0, /device:TPU:1, one launch (start us, length us, event | category | flops | bytes accessed | tf_op | source)
XLA Modules:
  0.0 76.2 jit_solution(15837005994373048394)
XLA Ops:
  0.6 73.3 %fused_layer.1 = (bf16[128,1024]{1,0:T(8,128)(2,1)}, f32[4,128]{1,0:T(4,128)}) custom-call(bf16[128,2048]{1,0:T(8,128)(2,1)} %tokens.1, bf16[2048]{0:T(1024)(128)(2,1)} %norm_gain.1, bf16[512,512]{1,0:T(8,128)(2,1)} %query_down.1, bf16[512]{0:T(512)(128)(2,1)} %query_gain.1, bf16[2048,256]{1,0:T(8,128)(2,1)} %latent_down.1, bf16[256]{0:T(256)(128)(2,1)} %latent_gain.1, ...), custom_call_target="tpu_custom_call" | custom-call | tf_op jit(solution)/shard_map/fused_layer/pallas_call | solution.py:705
  74.0 0.0 copy-start
  74.0 1.7 %copy.21 = bf16[128,1024]{1,0:T(8,128)(2,1)} copy(bf16[128,1024]{1,0:T(8,128)(2,1)} %get-tuple-element.4) | data formatting | bytes 524288
  75.7 0.0 copy-done
  75.7 0.6 copy.22
Async XLA Ops:
  74.0 1.7 %copy-start = (f32[4,128]{1,0:T(4,128)S(1)}, f32[4,128]{1,0:T(4,128)}, u32[]{:S(2)}) copy-start(f32[4,128]{1,0:T(4,128)} %get-tuple-element.5) | copy-start | bytes 6148
where the time goes:
time: 76.6 us; the launch traced here: 76.2 us
  Pallas kernels  73.3 us (96%)
  local copies, waits for them, and re-layouts  2.25 us (3%)
    pallas_call x1, Pallas kernels, fused_device(): pl.pallas_call(functools.partial(fused_kernel, n_sp), out_shape=(jax.Shap...  73.3 us
    unnamed x4, local copies, waits for them, and re-layouts  2.25 us

commit v1 on v0

v1 whole, which is shorter than its diff:
```python
import functools

import jax
import jax.numpy as jnp
import numpy as np
from jax import lax
from jax.experimental import pallas as pl
from jax.experimental.pallas import tpu as pltpu
from jax.sharding import PartitionSpec as P

NOPE = 128
ROPE = 64
VDIM = 128
KVR = 256
CH = 1024
GROUPS = 8
GRID_W = 64


norm_eps = 1e-06
rope_base = 10000.0
far_below = -1e30


def padded_2(block, sides, width):
    for axis, dim in sides:
        count = lax.axis_size(axis)
        forward = [(i, i + 1) for i in range(count - 1)]
        backward = [(target, source) for source, target in forward]
        low = lax.ppermute(
            lax.slice_in_dim(block, block.shape[dim] - width, None, axis=dim), axis, forward
        )
        high = lax.ppermute(lax.slice_in_dim(block, 0, width, axis=dim), axis, backward)
        block = jnp.concatenate([low, block, high], axis=dim)
    return block


def rms_scale(values, scale_gain):
    inv_rms = lax.rsqrt(jnp.mean(values * values, axis=-1, keepdims=True) + norm_eps)
    return values * inv_rms * scale_gain.astype(jnp.float32)


def angles_for(positions, rope_size):
    quarter = rope_size // 4
    inverse = rope_base ** (-jnp.arange(quarter, dtype=jnp.float32) / quarter)
    grid_row = (positions // GRID_W).astype(jnp.float32)
    grid_col = (positions % GRID_W).astype(jnp.float32)
    return jnp.concatenate([grid_row[:, None] * inverse, grid_col[:, None] * inverse], axis=-1)


def rotate(values, angles):
    half_size = values.shape[-1] // 2
    front_half = values[..., :half_size]
    back_half = values[..., half_size:]
    cosine = jnp.cos(angles)
    sine_part = jnp.sin(angles)
    return jnp.concatenate(
        [front_half * cosine - back_half * sine_part, back_half * cosine + front_half * sine_part],
        axis=-1,
    )


def key_block(normed, latent_down, latent_gain, rope_down, positions):
    latent = jnp.dot(normed, latent_down, preferred_element_type=jnp.float32)
    latent = rms_scale(latent, latent_gain).astype(jnp.bfloat16)
    rope_key = jnp.dot(normed, rope_down, preferred_element_type=jnp.float32)
    rope_key = rotate(rope_key, angles_for(positions, rope_key.shape[-1])).astype(jnp.bfloat16)
    return jnp.concatenate([latent, rope_key], axis=1)


def per_device(
    tokens,
    norm_gain,
    query_down,
    query_gain,
    latent_down,
    latent_gain,
    rope_down,
    query_up,
    key_up,
    value_up,
    glu_value,
    glu_gate,
    conv_taps,
    group_gain,
    head_proj,
    channel_proj,
):
    tok_count = tokens.shape[0]
    reach_rows = conv_taps.shape[0] // 2
    head_count = key_up.shape[1] // NOPE
    normed = rms_scale(tokens.astype(jnp.float32), norm_gain).astype(jnp.bfloat16)
    offsets = lax.axis_index("sp") * tok_count + jnp.arange(tok_count, dtype=jnp.int32)
    query_latent = jnp.dot(
        normed,
        lax.all_gather(query_down, "sp", axis=0, tiled=True),
        preferred_element_type=jnp.float32,
    )
    value_in = jnp.dot(
        normed,
        lax.all_gather(glu_value, "sp", axis=0, tiled=True),
        preferred_element_type=jnp.float32,
    )
    gate_in = jnp.dot(
        normed,
        lax.all_gather(glu_gate, "sp", axis=0, tiled=True),
        preferred_element_type=jnp.float32,
    )
    latent_query = rms_scale(query_latent, query_gain).astype(jnp.bfloat16)
    query_all = jnp.dot(latent_query, query_up, preferred_element_type=jnp.float32).reshape(
        tok_count, head_count, NOPE + ROPE
    )
    query_plain = query_all[:, :, :NOPE].astype(jnp.bfloat16)
    query_rope = rotate(query_all[:, :, NOPE:], angles_for(offsets, ROPE)[:, None, :]).astype(
        jnp.bfloat16
    )
    absorbed = jnp.einsum(
        "thd,rhd->htr",
        query_plain,
        key_up.reshape(KVR, head_count, NOPE),
        preferred_element_type=jnp.float32,
    ).astype(jnp.bfloat16)
    queries = jnp.concatenate([absorbed, jnp.transpose(query_rope, (1, 0, 2))], axis=-1)
    score_scale = (NOPE + ROPE) ** (-0.5)
    half_rows = tok_count // lax.axis_size("tp")
    first_row = lax.axis_index("tp") * half_rows
    own_rows = lax.dynamic_slice_in_dim(normed, first_row, half_rows, 0)
    own_positions = lax.dynamic_slice_in_dim(offsets, first_row, half_rows, 0)
    own_keys = key_block(own_rows, latent_down, latent_gain, rope_down, own_positions)
    block_keys = lax.all_gather(own_keys, ("sp", "tp"), axis=0, tiled=True)
    row_max = jnp.full((head_count, tok_count), far_below, jnp.float32)
    scores = (
        jnp.einsum("hqc,kc->hqk", queries, block_keys, preferred_element_type=jnp.float32)
        * score_scale
    )
    new_max = jnp.maximum(row_max, jnp.max(scores, axis=2))
    weights = jnp.exp(scores - new_max[:, :, None])
    new_sum = jnp.sum(weights, axis=2)
    added = jnp.einsum(
        "hqk,kr->hqr",
        weights.astype(jnp.bfloat16),
        block_keys[:, :KVR],
        preferred_element_type=jnp.float32,
    )
    gated_rows = (value_in * jax.nn.sigmoid(gate_in)).astype(jnp.bfloat16)
    padded = padded_2(gated_rows, (("sp", 0),), reach_rows)
    filtered = padded[0:tok_count].astype(jnp.float32) * conv_taps[0].astype(jnp.float32)
    for tap_index in range(1, conv_taps.shape[0]):
        filtered = filtered + padded[tap_index : tap_index + tok_count].astype(
            jnp.float32
        ) * conv_taps[tap_index].astype(jnp.float32)
    grouped = filtered.reshape(tok_count, -1, CH // GROUPS)
    centred = grouped - jnp.mean(grouped, axis=-1, keepdims=True)
    spread = jnp.mean(centred * centred, axis=-1, keepdims=True)
    normal_groups = (centred * lax.rsqrt(spread + norm_eps)).reshape(tok_count, -1)
    conv_branch = jax.nn.silu(normal_groups * group_gain.astype(jnp.float32)).astype(jnp.bfloat16)
    attended = (added / new_sum[:, :, None]).astype(jnp.bfloat16)
    log_weight = new_max + jnp.log(new_sum)
    head_out = jnp.einsum(
        "htr,rhv->thv",
        attended,
        value_up.reshape(KVR, head_count, VDIM),
        preferred_element_type=jnp.float32,
    )
    head_out = head_out.reshape(tok_count, head_count * VDIM).astype(jnp.bfloat16)
    mixed_in = jnp.concatenate([head_out, conv_branch], axis=1)
    out_weight = jnp.concatenate([head_proj, channel_proj], axis=0)
    partial_terms = jnp.dot(
        mixed_in,
        lax.all_gather(out_weight, "sp", axis=1, tiled=True),
        preferred_element_type=jnp.float32,
    )
    mixed_out = lax.psum_scatter(
        partial_terms.astype(jnp.bfloat16), "tp", scatter_dimension=1, tiled=True
    )
    return (mixed_out, log_weight)


LANES = 128
MESH = pl.DeviceIdType.MESH
F32 = jnp.float32
BF16 = jnp.bfloat16
LOW, HIGH, FWD = range(3)
Q, K, V, W, H, C = range(6)


def rope_tables(length):
    quarter = ROPE // 4
    inverse = np.float32(rope_base) ** (-np.arange(quarter, dtype=np.float32) / np.float32(quarter))
    positions = np.arange(length)
    row = (positions // GRID_W).astype(np.float32)[:, None] * inverse
    col = (positions % GRID_W).astype(np.float32)[:, None] * inverse
    angles = np.concatenate([row, col], axis=1).astype(np.float32)
    cosine, sine = np.cos(angles), np.sin(angles)
    tables = np.zeros((3, length, LANES), np.float32)
    half = ROPE // 2
    tables[0, :, :half] = cosine
    tables[0, :, half:ROPE] = cosine
    tables[1, :, :half] = -sine
    tables[2, :, half:ROPE] = sine
    return tables


def dot(a, b):
    return jnp.dot(a, b, preferred_element_type=F32)


def row_of(ref):
    return ref[...].reshape(1, -1)


def dot_nt(a, b):
    return lax.dot_general(a, b, (((1,), (1,)), ((), ())), preferred_element_type=F32)


def fused_kernel(
    n_sp,
    tokens, norm_gain, query_down, query_gain, latent_down, latent_gain, rope_down, query_up,
    key_up, value_up, glu_value, glu_gate, conv_taps, group_gain, head_proj, channel_proj, tables,
    out, log_out,
    w_q, w_g, w_o, tok_v, lat_v, rope_v, qup_v, kup_v, vup_v, tab_v,
    normed, keys, key_tmp, q_out, q_lat, q_scr, g_acc, gated, low_rows, high_rows, padded,
    mixed, parts, peer_parts, final, out_v,
    load_sem, z_recv, z_send, pair_recv, pair_send, n_recv, n_send, np_recv, np_send, q_recv, q_send,
    head_recv, head_send, halo_recv, halo_send, conv_recv, conv_send, p_recv, p_send, fin_recv, fin_send,
    corner_sem,
):
    z = lax.axis_index("sp")
    c = lax.axis_index("fs")
    t = lax.axis_index("tp")
    peer = 1 - t
    c_x = c + 1 - 2 * (c % 2)
    c_y = (c + 2) % 4
    c_d = 3 - c
    others = (c_x, c_y, c_d)
    n_fs = normed.shape[0]
    n_tp = 2
    rows, width = tokens.shape
    depth, q_cols = w_q.shape[1:]
    cols = w_g.shape[2] // 2
    heads = key_up.shape[1] // NOPE
    head_rows = head_proj.shape[0]
    out_rows, out_cols = w_o.shape[1:]
    half_width = width // n_tp
    per_core = n_fs // n_tp
    half_sp = n_sp // n_tp

    def lanes_at(index, size):
        return pl.ds(pl.multiple_of(index * size, LANES), size)

    loads = {}

    def load(name, src, dst):
        copy = pltpu.make_async_copy(src, dst, load_sem.at[len(loads)])
        copy.start()
        loads[name] = copy

    load("tok", tokens, tok_v)
    load("wq", query_down.at[:, lanes_at(c, q_cols)], w_q.at[z])
    load("wv", glu_value.at[:, lanes_at(c, cols)], w_g.at[z, :, pl.ds(0, cols)])
    load("wt", glu_gate.at[:, lanes_at(c, cols)], w_g.at[z, :, pl.ds(cols, cols)])
    load("lat", latent_down, lat_v)
    load("rope", rope_down, rope_v)
    load("tab", tables.at[:, pl.ds(pl.multiple_of(z * rows, LANES), rows), :], tab_v)
    load("hp", head_proj.at[:, lanes_at(c, out_cols)], w_o.at[z, pl.ds(0, head_rows), :])
    load("cp", channel_proj.at[:, lanes_at(c, out_cols)], w_o.at[z, pl.ds(head_rows, out_rows - head_rows), :])
    load("qup", query_up, qup_v)
    load("kup", key_up, kup_v)
    load("vup", value_up, vup_v)

    barrier = pltpu.get_barrier_semaphore()
    sides = [{"fs": c_x}, {"fs": c_y}, {"tp": peer}]
    for partner in sides:
        pl.semaphore_signal(barrier, inc=1, device_id=partner, device_id_type=MESH)

    @pl.when(z > 0)
    def _():
        pl.semaphore_signal(barrier, inc=1, device_id={"sp": z - 1}, device_id_type=MESH)

    @pl.when(z < n_sp - 1)
    def _():
        pl.semaphore_signal(barrier, inc=1, device_id={"sp": z + 1}, device_id_type=MESH)

    loads["tok"].wait()
    values = tok_v[...].astype(F32)
    normed[c] = rms_scale(values, row_of(norm_gain)).astype(BF16)
    for name in ("wq", "wv", "wt"):
        loads[name].wait()

    ends = (z == 0).astype(jnp.int32) + (z == n_sp - 1).astype(jnp.int32)
    pl.semaphore_wait(barrier, len(sides) + 2 - ends)
    pl.semaphore_signal(corner_sem, inc=1, device_id={"fs": c_x}, device_id_type=MESH)

    def remote(src, dst, send_sem, recv_sem, device):
        return pltpu.make_async_remote_copy(
            src_ref=src, dst_ref=dst, send_sem=send_sem, recv_sem=recv_sem,
            device_id=device, device_id_type=MESH,
        )

    q_half = depth // n_tp
    g_half = depth // 2
    k_half = rows // n_tp

    def half(first, size):
        return pl.ds(pl.multiple_of(first * size, 16), size)

    def block(u, shard, side=t):
        if u == Q:
            return w_q.at[shard, half(side, q_half), :]
        if u == K:
            return keys.at[shard, half(side, k_half), :]
        if u == V:
            return w_g.at[shard, pl.ds(0, g_half), :]
        if u == W:
            return w_g.at[shard, pl.ds(g_half, depth - g_half), :]
        if u == H:
            return w_o.at[shard, pl.ds(0, head_rows), :]
        return w_o.at[shard, pl.ds(head_rows, out_rows - head_rows), :]

    def z_copy(u, shard, kind, target):
        ref = block(u, shard)
        return remote(ref, ref, z_send.at[u, shard, kind], z_recv.at[u, shard], {"sp": target})

    def own(u, action):
        @pl.when(z > 0)
        def _():
            action(z_copy(u, z, LOW, z - 1))

        @pl.when(z < n_sp - 1)
        def _():
            action(z_copy(u, z, HIGH, z + 1))

    def send_own(u):
        own(u, lambda copy: copy.start())

    nearest = jnp.minimum(z, n_sp - 1 - z)
    arrivals = []
    for k in range(n_sp - 1):
        both = k < 2 * nearest
        distance = jnp.where(both, k // 2 + 1, k - nearest + 1)
        from_low = jnp.where(both, 1 - k % 2, (2 * z > n_sp - 1).astype(jnp.int32))
        arrivals.append((z - distance * (2 * from_low - 1), z + 2 * from_low - 1))

    def forwards(k):
        target = arrivals[k][1]
        return (target >= 0) & (target < n_sp)

    def relay(u, k):
        shard, target = arrivals[k]

        @pl.when(forwards(k))
        def _():
            copy = z_copy(u, shard, FWD, target)
            copy.wait_recv()
            copy.start()

    def settle(u, k):
        @pl.when(jnp.logical_not(forwards(k)))
        def _():
            z_copy(u, arrivals[k][0], FWD, jnp.where(z > 0, z - 1, z + 1)).wait_recv()

    def pair(u, shard, side):
        ref = block(u, shard, side)
        return remote(ref, ref, pair_send.at[u, shard], pair_recv.at[u, shard], {"tp": peer})

    def share(u, k):
        settle(u, k)
        pair(u, arrivals[k][0], t).start()

    def n_copy(i):
        ref = normed.at[c, :, lanes_at(t, half_width)]
        return remote(ref, ref, n_send.at[i], n_recv.at[i], {"fs": others[i]})

    def n_pair(i, side):
        ref = normed.at[others[i], :, lanes_at(side, half_width)]
        return remote(ref, ref, np_send.at[i], np_recv.at[i], {"tp": peer})

    def share_normed(i):
        n_copy(i).wait_recv()
        n_pair(i, t).start()

    send_own(Q)
    send_own(V)
    n_copy(0).start()
    n_copy(1).start()
    pl.semaphore_wait(corner_sem, 1)
    n_copy(2).start()

    def rotate_lanes(v):
        step = ROPE // 2
        return (
            v * tab_v[0] + pltpu.roll(v, LANES - step, 1) * tab_v[1] + pltpu.roll(v, step, 1) * tab_v[2]
        )

    loads["lat"].wait()
    own_normed = normed[c]
    latent = rms_scale(dot(own_normed, lat_v[...]), row_of(latent_gain))
    keys[z, :, 0:KVR] = latent.astype(BF16)
    loads["rope"].wait()
    loads["tab"].wait()
    key_tmp[...] = jnp.zeros_like(key_tmp)
    key_tmp[:, 0:ROPE] = dot_nt(own_normed, rope_v[...])
    keys[z, :, KVR : KVR + LANES] = rotate_lanes(key_tmp[...]).astype(BF16)
    send_own(K)

    last = n_sp - 2
    for u in (Q, K):
        for k in range(last):
            relay(u, k)
    send_own(W)
    share(Q, 0)
    share(K, 0)
    for k in range(last):
        relay(V, k)
    share_normed(0)
    share_normed(1)
    for u in (Q, K):
        relay(u, last)
    for k in range(1, last):
        share(Q, k)
        share(K, k)
    for k in range(last):
        relay(W, k)
    share_normed(2)
    share(Q, last)
    share(K, last)
    relay(V, last)

    for i in range(len(others)):
        n_pair(i, peer).wait_recv()
    for k in range(n_sp - 1):
        pair(Q, arrivals[k][0], peer).wait_recv()
    seqs = normed[pl.ds(per_core * t, per_core)].reshape(per_core * rows, width)
    q_out[...] = dot(seqs, w_q[...].reshape(n_sp * depth, q_cols)).reshape(per_core, rows, q_cols)

    def q_copies(i):
        seq = per_core * t + i
        return seq, [
            remote(q_out.at[i], q_lat.at[c], q_send.at[i, j], q_recv.at[c], {"fs": seq, "tp": core})
            for j, core in enumerate((t, peer))
        ]

    for i in range(per_core):
        seq, (same, other) = q_copies(i)
        other.start()

        @pl.when(seq != c)
        def _():
            same.start()

        @pl.when(seq == c)
        def _():
            q_lat[c] = q_out[i]

    def add_shard(shard, first=False):
        rows_in = normed[:, :, lanes_at(shard, depth)].reshape(n_fs * rows, depth)
        term = dot(rows_in, w_g[shard])
        g_acc[...] = term if first else g_acc[...] + term

    add_shard(z, True)
    relay(W, last)
    for name in ("hp", "cp", "qup", "kup", "vup"):
        loads[name].wait()
    send_own(H)
    send_own(C)
    for u in (V, W):
        settle(u, 0)
    add_shard(arrivals[0][0])

    for source in range(n_fs):
        @pl.when((c != source) | (t != c // per_core))
        def _():
            remote(q_out.at[0], q_lat.at[source], q_send.at[0, 0], q_recv.at[source], {"tp": peer}).wait_recv()

    whole_q = jnp.concatenate([q_lat[i] for i in range(n_fs)], axis=1)
    latent_query = rms_scale(whole_q, row_of(query_gain)).astype(BF16)
    q_scr[...] = dot(latent_query, qup_v[...])
    for k in range(n_sp - 1):
        pair(K, arrivals[k][0], peer).wait_recv()

    def attend(h, shifted):
        start = h * (NOPE + ROPE)
        source = q_scr[...]
        if start % LANES:
            source, start = shifted, start - ROPE
        plain = source[:, start : start + NOPE].astype(BF16)
        rope_part = rotate_lanes(source[:, start + NOPE : start + NOPE + LANES]).astype(BF16)
        absorbed = dot_nt(plain, kup_v[:, h * NOPE : (h + 1) * NOPE]).astype(BF16)
        query = jnp.concatenate([absorbed, rope_part], axis=1)
        all_keys = keys[...].reshape(n_sp * rows, KVR + LANES)
        scores = dot_nt(query, all_keys) * (NOPE + ROPE) ** (-0.5)
        row_max = jnp.max(scores, axis=1, keepdims=True)
        weights = jnp.exp(scores - row_max)
        total = jnp.sum(weights, axis=1, keepdims=True)
        added = dot(weights.astype(BF16), all_keys[:, 0:KVR])
        attended = (added / total).astype(BF16)
        head_out = dot(attended, vup_v[:, h * VDIM : (h + 1) * VDIM])
        mixed[c, :, h * VDIM : (h + 1) * VDIM] = head_out.astype(BF16)
        return row_max + jnp.log(total)

    def head_copy(h, i):
        ref = mixed.at[c, :, pl.ds(h * VDIM, VDIM)]
        return remote(ref, ref, head_send.at[h, i], head_recv.at[h, i], {"fs": others[i]})

    whole = q_scr[...]
    shifted = pltpu.roll(whole, whole.shape[1] - ROPE, 1)
    lane = lax.broadcasted_iota(jnp.int32, (rows, LANES), 1)
    logs = jnp.zeros((rows, LANES), F32)
    relays = {1: [(H, 0)], 2: [(H, 1), (C, 0)], 3: [(C, 1)]}
    for h in range(heads):
        logs = jnp.where(lane == h, attend(h, shifted), logs)
        for i in range(len(others)):
            head_copy(h, i).start()
        for u, k in relays.get(h, []):
            relay(u, k)
    log_out[...] = jnp.transpose(logs)[0:heads, :]

    for k in range(1, n_sp - 1):
        for u in (V, W):
            settle(u, k)
        add_shard(arrivals[k][0])

    halo = low_rows.shape[1]
    reach = conv_taps.shape[0] // 2
    acc = g_acc[...]
    gated[...] = (acc[:, 0:cols] * jax.nn.sigmoid(acc[:, cols : 2 * cols])).astype(BF16).reshape(n_fs, rows, cols)
    up_copy = remote(
        gated.at[:, pl.ds(rows - halo, halo), :], low_rows, halo_send.at[0], halo_recv.at[0], {"sp": z + 1}
    )
    down_copy = remote(
        gated.at[:, pl.ds(0, halo), :], high_rows, halo_send.at[1], halo_recv.at[1], {"sp": z - 1}
    )

    @pl.when(z < n_sp - 1)
    def _():
        up_copy.start()

    @pl.when(z > 0)
    def _():
        down_copy.start()

    padded[:, halo : halo + rows, :] = gated[...].astype(F32)
    relay(H, last)

    @pl.when(z > 0)
    def _():
        up_copy.wait_recv()
        padded[:, 0:halo, :] = low_rows[...].astype(F32)

    @pl.when(z == 0)
    def _():
        padded[:, 0:halo, :] = jnp.zeros((n_fs, halo, cols), F32)

    @pl.when(z < n_sp - 1)
    def _():
        down_copy.wait_recv()
        padded[:, halo + rows : 2 * halo + rows, :] = high_rows[...].astype(F32)

    @pl.when(z == n_sp - 1)
    def _():
        padded[:, halo + rows : 2 * halo + rows, :] = jnp.zeros((n_fs, halo, cols), F32)

    def conv_copy(s, i):
        ref = mixed.at[s, :, pl.ds(pl.multiple_of(head_rows + c * cols, LANES), cols)]
        return remote(ref, ref, conv_send.at[s, i], conv_recv.at[s, i], {"fs": others[i]})

    own_lanes = lanes_at(c, cols)
    taps = conv_taps[:, own_lanes].astype(F32)
    all_gains = row_of(group_gain).astype(F32)
    gains = all_gains[:, 0:cols]
    for i in range(1, n_fs):
        gains = jnp.where(c == i, all_gains[:, i * cols : (i + 1) * cols], gains)
    for s in range(n_fs):
        filtered = jnp.zeros((rows, cols), F32)
        for j in range(conv_taps.shape[0]):
            first = halo - reach + j
            filtered = filtered + padded[s, first : first + rows, :] * taps[j : j + 1, :]
        centred = filtered - jnp.mean(filtered, axis=1, keepdims=True)
        spread = jnp.mean(centred * centred, axis=1, keepdims=True)
        branch = centred * lax.rsqrt(spread + norm_eps) * gains
        branch = branch * jax.nn.sigmoid(branch)
        mixed[s, :, pl.ds(pl.multiple_of(head_rows + c * cols, LANES), cols)] = branch.astype(BF16)
        for i in range(len(others)):
            conv_copy(s, i).start()
        if s == 1:
            relay(C, last)

    for i in range(len(others)):
        for h in range(heads):
            head_copy(h, i).wait_recv()
    for s in range(n_fs):
        for i in range(len(others)):
            conv_copy(s, i).wait_recv()

    def p_copy(i):
        return remote(
            parts.at[peer * half_sp + i], peer_parts.at[i], p_send.at[i], p_recv.at[i], {"tp": peer}
        )

    def fin_copy(i, j):
        return remote(
            final.at[i, pl.ds(pl.multiple_of(others[j] * rows, LANES), rows), :],
            out_v.at[:, pl.ds(pl.multiple_of(i * n_fs * out_cols + c * out_cols, LANES), out_cols)],
            fin_send.at[i, j], fin_recv.at[i, j], {"fs": others[j]},
        )

    def add_part(shard):
        part = dot(mixed[...].reshape(n_fs * rows, out_rows), w_o[shard])
        parts[shard] = part.astype(BF16)
        for i in range(half_sp):
            @pl.when(shard == peer * half_sp + i)
            def _():
                p_copy(i).start()

    def finish(shard):
        for i in range(half_sp):
            @pl.when(shard == t * half_sp + i)
            def _():
                p_copy(i).wait_recv()
                total = parts[t * half_sp + i].astype(F32) + peer_parts[i].astype(F32)
                final[i] = total.astype(BF16)
                for j in range(len(others)):
                    fin_copy(i, j).start()
                out_v[:, pl.ds(pl.multiple_of(i * n_fs * out_cols + c * out_cols, LANES), out_cols)] = final[
                    i, pl.ds(pl.multiple_of(c * rows, LANES), rows), :
                ]

    shards = [z] + [shard for shard, _ in arrivals]
    for k, shard in enumerate(shards):
        if k:
            settle(H, k - 1)
            settle(C, k - 1)
        add_part(shard)
        if k:
            finish(shards[k - 1])
    finish(shards[-1])

    for u in (Q, K, V, W, H, C):
        own(u, lambda copy: copy.wait_send())
        for k in range(n_sp - 1):
            shard, target = arrivals[k]

            @pl.when(forwards(k))
            def _():
                z_copy(u, shard, FWD, target).wait_send()

            if u in (Q, K):
                pair(u, shard, t).wait_send()
    for i in range(len(others)):
        n_copy(i).wait_send()
        n_pair(i, t).wait_send()
        for h in range(heads):
            head_copy(h, i).wait_send()
        for s in range(n_fs):
            conv_copy(s, i).wait_send()
    for i in range(per_core):
        seq, (same, other) = q_copies(i)
        other.wait_send()

        @pl.when(seq != c)
        def _():
            same.wait_send()

    @pl.when(z < n_sp - 1)
    def _():
        up_copy.wait_send()

    @pl.when(z > 0)
    def _():
        down_copy.wait_send()

    for i in range(half_sp):
        p_copy(i).wait_send()
        for j in range(len(others)):
            fin_copy(i, j).wait()
    out[...] = out_v[...]


def fused_device(n_sp, n_fs, *args):
    (tokens, norm_gain, query_down, query_gain, latent_down, latent_gain, rope_down, query_up,
     key_up, value_up, glu_value, glu_gate, conv_taps, group_gain, head_proj, channel_proj) = args
    rows, width = tokens.shape
    depth, q_rank = query_down.shape
    cols = glu_value.shape[1] // n_fs
    heads = key_up.shape[1] // NOPE
    out_rows = head_proj.shape[0] + channel_proj.shape[0]
    out_cols = head_proj.shape[1] // n_fs
    q_cols = q_rank // n_fs
    halo = (conv_taps.shape[0] // 2 + 15) // 16 * 16
    tables = jnp.asarray(rope_tables(n_sp * rows))
    vmem = pl.BlockSpec(memory_space=pltpu.VMEM)
    hbm = pl.BlockSpec(memory_space=pltpu.HBM)
    operands = [
        (tokens, hbm), (norm_gain, vmem), (query_down, hbm), (query_gain, vmem),
        (latent_down, hbm), (latent_gain, vmem), (rope_down.T, hbm), (query_up, hbm),
        (key_up, hbm), (value_up, hbm), (glu_value, hbm), (glu_gate, hbm), (conv_taps, vmem),
        (group_gain, vmem), (head_proj, hbm), (channel_proj, hbm), (tables, hbm),
    ]
    like = lambda a: pltpu.VMEM(a.shape, a.dtype)
    dma = pltpu.SemaphoreType.DMA
    half_sp = n_sp // 2
    scratch = [
        pltpu.VMEM((n_sp, depth, q_cols), BF16),
        pltpu.VMEM((n_sp, depth, 2 * cols), BF16),
        pltpu.VMEM((n_sp, out_rows, out_cols), BF16),
        like(tokens), like(latent_down), pltpu.VMEM(rope_down.shape[::-1], BF16), like(query_up), like(key_up), like(value_up),
        pltpu.VMEM((3, rows, LANES), F32),
        pltpu.VMEM((n_fs, rows, width), BF16),
        pltpu.VMEM((n_sp, rows, KVR + LANES), BF16),
        pltpu.VMEM((rows, LANES), F32),
        pltpu.VMEM((n_fs // 2, rows, q_cols), F32),
        pltpu.VMEM((n_fs, rows, q_cols), F32),
        pltpu.VMEM((rows, query_up.shape[1]), F32),
        pltpu.VMEM((n_fs * rows, 2 * cols), F32),
        pltpu.VMEM((n_fs, rows, cols), BF16),
        pltpu.VMEM((n_fs, halo, cols), BF16),
        pltpu.VMEM((n_fs, halo, cols), BF16),
        pltpu.VMEM((n_fs, rows + 2 * halo, cols), F32),
        pltpu.VMEM((n_fs, rows, out_rows), BF16),
        pltpu.VMEM((n_sp, n_fs * rows, out_cols), BF16),
        pltpu.VMEM((half_sp, n_fs * rows, out_cols), BF16),
        pltpu.VMEM((half_sp, n_fs * rows, out_cols), BF16),
        pltpu.VMEM((rows, half_sp * n_fs * out_cols), BF16),
        dma((12,)), dma((6, n_sp)), dma((6, n_sp, 3)), dma((2, n_sp)), dma((2, n_sp)),
        dma((3,)), dma((3,)), dma((3,)), dma((3,)), dma((n_fs,)), dma((n_fs // 2, 2)),
        dma((heads, 3)), dma((heads, 3)), dma((2,)), dma((2,)), dma((n_fs, 3)), dma((n_fs, 3)),
        dma((half_sp,)), dma((half_sp,)), dma((half_sp, 3)), dma((half_sp, 3)),
        pltpu.SemaphoreType.REGULAR,
    ]
    return pl.pallas_call(
        functools.partial(fused_kernel, n_sp),
        out_shape=(
            jax.ShapeDtypeStruct((rows, half_sp * n_fs * out_cols), BF16),
            jax.ShapeDtypeStruct((heads, rows), F32),
        ),
        in_specs=[spec for _, spec in operands],
        out_specs=(vmem, vmem),
        scratch_shapes=scratch,
        compiler_params=pltpu.CompilerParams(
            collective_id=0, has_side_effects=True, vmem_limit_bytes=63 * 1024 * 1024
        ),
        name="fused_layer",
    )(*[value for value, _ in operands])


def solution(mesh):
    in_specs = (
        P(("fs", "sp"), None),
        P(),
        P("sp", None),
        P(),
        P(),
        P(),
        P(),
        P(None, "tp"),
        P(None, "tp"),
        P(None, "tp"),
        P("sp", "tp"),
        P("sp", "tp"),
        P(None, "tp"),
        P("tp"),
        P("tp", "sp"),
        P("tp", "sp"),
    )
    out_specs = (P(("fs", "sp"), "tp"), P("tp", ("fs", "sp")))
    body = per_device
    if mesh.shape["fs"] == 4 and mesh.shape["tp"] == 2 and mesh.shape["sp"] == 4:
        body = functools.partial(fused_device, mesh.shape["sp"], mesh.shape["fs"])
    return jax.shard_map(
        body, mesh=mesh, in_specs=in_specs, out_specs=out_specs, check_vma=False
    )
```

time: 76.6 us -> 62.5 us (0.82)
  Pallas kernels: 73.3 us -> 59.4 us
    pallas_call x1, Pallas kernels: 73.3 us -> 59.4 us  [fused_device(): pl.pallas_call(functools.partial(fused_kernel, n_sp), out_shape=(jax.Shap...]
where the time goes in v1:
time: 62.5 us; the launch traced here: 62.3 us
  Pallas kernels  59.4 us (95%)
  local copies, waits for them, and re-layouts  2.25 us (4%)
  between operations  0.65 us (1%)
    pallas_call x1, Pallas kernels, fused_device(): pl.pallas_call(functools.partial(fused_kernel, n_sp), out_shape=(jax.Shap...  59.4 us
    unnamed x4, local copies, waits for them, and re-layouts  2.25 us

profile of v1, /device:TPU:1, one launch (start us, length us, event | category | flops | bytes accessed | tf_op | source)
XLA Modules:
  0.0 62.3 jit_solution(16446249631251134372)
XLA Ops:
  0.6 59.4 %fused_layer.1 = (bf16[128,1024]{1,0:T(8,128)(2,1)}, f32[4,128]{1,0:T(4,128)}) custom-call(bf16[128,2048]{1,0:T(8,128)(2,1)} %tokens.1, bf16[2048]{0:T(1024)(128)(2,1)} %norm_gain.1, bf16[512,512]{1,0:T(8,128)(2,1)} %query_down.1, bf16[512]{0:T(512)(128)(2,1)} %query_gain.1, bf16[2048,256]{1,0:T(8,128)(2,1)} %latent_down.1, bf16[256]{0:T(256)(128)(2,1)} %latent_gain.1, ...), custom_call_target="tpu_custom_call" | custom-call | tf_op jit(solution)/shard_map/fused_layer/pallas_call | solution.py:730
  60.1 0.0 copy-start
  60.1 1.7 %copy.21 = bf16[128,1024]{1,0:T(8,128)(2,1)} copy(bf16[128,1024]{1,0:T(8,128)(2,1)} %get-tuple-element.4) | data formatting | bytes 524288
  61.8 0.0 copy-done
  61.8 0.6 copy.22
Async XLA Ops:
  60.1 1.7 %copy-start = (f32[4,128]{1,0:T(4,128)S(1)}, f32[4,128]{1,0:T(4,128)}, u32[]{:S(2)}) copy-start(f32[4,128]{1,0:T(4,128)} %get-tuple-element.5) | copy-start | bytes 6148

commit v2 on v1

--- a/solution.py
+++ b/solution.py
@@ -215,14 +215,15 @@
 
 def fused_kernel(
     n_sp,
-    tokens, norm_gain, query_down, query_gain, latent_down, latent_gain, rope_down, query_up,
-    key_up, value_up, glu_value, glu_gate, conv_taps, group_gain, head_proj, channel_proj, tables,
+    tokens, norm_gain_in, query_down, query_gain_in, latent_down, latent_gain_in, rope_down, query_up,
+    key_up, value_up, glu_value, glu_gate, taps_in, group_gain_in, head_proj, channel_proj, tables,
     out, log_out,
+    norm_gain, query_gain, latent_gain, conv_taps, group_gain, log_v,
     w_q, w_g, w_o, tok_v, lat_v, rope_v, qup_v, kup_v, vup_v, tab_v,
     normed, keys, key_tmp, q_out, q_lat, q_scr, g_acc, gated, low_rows, high_rows, padded,
-    mixed, parts, peer_parts, final, out_v,
+    mixed, parts, placed, out_v,
     load_sem, z_recv, z_send, pair_recv, pair_send, n_recv, n_send, np_recv, np_send, q_recv, q_send,
-    head_recv, head_send, halo_recv, halo_send, conv_recv, conv_send, p_recv, p_send, fin_recv, fin_send,
+    head_recv, head_send, halo_recv, halo_send, conv_recv, conv_send, fin_recv, fin_send, out_sem,
     corner_sem,
 ):
     z = lax.axis_index("sp")
@@ -248,6 +249,19 @@
     def lanes_at(index, size):
         return pl.ds(pl.multiple_of(index * size, LANES), size)
 
+    barrier = pltpu.get_barrier_semaphore()
+    sides = [{"fs": c_x}, {"fs": c_y}, {"tp": peer}]
+    for partner in sides:
+        pl.semaphore_signal(barrier, inc=1, device_id=partner, device_id_type=MESH)
+
+    @pl.when(z > 0)
+    def _():
+        pl.semaphore_signal(barrier, inc=1, device_id={"sp": z - 1}, device_id_type=MESH)
+
+    @pl.when(z < n_sp - 1)
+    def _():
+        pl.semaphore_signal(barrier, inc=1, device_id={"sp": z + 1}, device_id_type=MESH)
+
     loads = {}
 
     def load(name, src, dst):
@@ -256,6 +270,7 @@
         loads[name] = copy
 
     load("tok", tokens, tok_v)
+    load("ng", norm_gain_in, norm_gain)
     load("wq", query_down.at[:, lanes_at(c, q_cols)], w_q.at[z])
     load("wv", glu_value.at[:, lanes_at(c, cols)], w_g.at[z, :, pl.ds(0, cols)])
     load("wt", glu_gate.at[:, lanes_at(c, cols)], w_g.at[z, :, pl.ds(cols, cols)])
@@ -267,21 +282,13 @@
     load("qup", query_up, qup_v)
     load("kup", key_up, kup_v)
     load("vup", value_up, vup_v)
-
-    barrier = pltpu.get_barrier_semaphore()
-    sides = [{"fs": c_x}, {"fs": c_y}, {"tp": peer}]
-    for partner in sides:
-        pl.semaphore_signal(barrier, inc=1, device_id=partner, device_id_type=MESH)
-
-    @pl.when(z > 0)
-    def _():
-        pl.semaphore_signal(barrier, inc=1, device_id={"sp": z - 1}, device_id_type=MESH)
-
-    @pl.when(z < n_sp - 1)
-    def _():
-        pl.semaphore_signal(barrier, inc=1, device_id={"sp": z + 1}, device_id_type=MESH)
+    load("qg", query_gain_in, query_gain)
+    load("lg", latent_gain_in, latent_gain)
+    load("taps", taps_in.at[:, lanes_at(c, cols)], conv_taps)
+    load("gg", group_gain_in, group_gain)
 
     loads["tok"].wait()
+    loads["ng"].wait()
     values = tok_v[...].astype(F32)
     normed[c] = rms_scale(values, row_of(norm_gain)).astype(BF16)
     for name in ("wq", "wv", "wt"):
@@ -383,8 +390,6 @@
     send_own(V)
     n_copy(0).start()
     n_copy(1).start()
-    pl.semaphore_wait(corner_sem, 1)
-    n_copy(2).start()
 
     def rotate_lanes(v):
         step = ROPE // 2
@@ -393,6 +398,7 @@
         )
 
     loads["lat"].wait()
+    loads["lg"].wait()
     own_normed = normed[c]
     latent = rms_scale(dot(own_normed, lat_v[...]), row_of(latent_gain))
     keys[z, :, 0:KVR] = latent.astype(BF16)
@@ -403,26 +409,30 @@
     keys[z, :, KVR : KVR + LANES] = rotate_lanes(key_tmp[...]).astype(BF16)
     send_own(K)
 
+    pl.semaphore_wait(corner_sem, 1)
+    n_copy(2).start()
+
     last = n_sp - 2
-    for u in (Q, K):
-        for k in range(last):
-            relay(u, k)
+    for k in range(last):
+        relay(Q, k)
     send_own(W)
+    for k in range(last):
+        relay(K, k)
     share(Q, 0)
-    share(K, 0)
+    relay(Q, last)
+    relay(K, last)
     for k in range(last):
         relay(V, k)
     share_normed(0)
     share_normed(1)
-    for u in (Q, K):
-        relay(u, last)
+    share(K, 0)
     for k in range(1, last):
         share(Q, k)
         share(K, k)
     for k in range(last):
         relay(W, k)
+    share(Q, last)
     share_normed(2)
-    share(Q, last)
     share(K, last)
     relay(V, last)
 
@@ -457,15 +467,42 @@
         term = dot(rows_in, w_g[shard])
         g_acc[...] = term if first else g_acc[...] + term
 
+    halo = low_rows.shape[1]
+    up_copy = remote(
+        gated.at[:, pl.ds(rows - halo, halo), :], low_rows, halo_send.at[0], halo_recv.at[0], {"sp": z + 1}
+    )
+    down_copy = remote(
+        gated.at[:, pl.ds(0, halo), :], high_rows, halo_send.at[1], halo_recv.at[1], {"sp": z - 1}
+    )
+
+    def gate():
+        for k in range(n_sp - 1):
+            for u in (V, W):
+                settle(u, k)
+            add_shard(arrivals[k][0])
+        acc = g_acc[...]
+        gated[...] = (acc[:, 0:cols] * jax.nn.sigmoid(acc[:, cols : 2 * cols])).astype(BF16).reshape(n_fs, rows, cols)
+
+        @pl.when(z < n_sp - 1)
+        def _():
+            up_copy.start()
+
+        @pl.when(z > 0)
+        def _():
+            down_copy.start()
+
+    inner = (z > 0) & (z < n_sp - 1)
     add_shard(z, True)
     relay(W, last)
-    for name in ("hp", "cp", "qup", "kup", "vup"):
+
+    @pl.when(inner)
+    def _():
+        gate()
+
+    for name in ("hp", "cp", "qup", "kup", "vup", "qg", "taps", "gg"):
         loads[name].wait()
     send_own(H)
     send_own(C)
-    for u in (V, W):
-        settle(u, 0)
-    add_shard(arrivals[0][0])
 
     for source in range(n_fs):
         @pl.when((c != source) | (t != c // per_core))
@@ -506,39 +543,22 @@
     shifted = pltpu.roll(whole, whole.shape[1] - ROPE, 1)
     lane = lax.broadcasted_iota(jnp.int32, (rows, LANES), 1)
     logs = jnp.zeros((rows, LANES), F32)
-    relays = {1: [(H, 0)], 2: [(H, 1), (C, 0)], 3: [(C, 1)]}
+    relays = {heads - 1: [(u, k) for u in (H, C) for k in range(last)]}
     for h in range(heads):
         logs = jnp.where(lane == h, attend(h, shifted), logs)
         for i in range(len(others)):
             head_copy(h, i).start()
         for u, k in relays.get(h, []):
             relay(u, k)
-    log_out[...] = jnp.transpose(logs)[0:heads, :]
-
-    for k in range(1, n_sp - 1):
-        for u in (V, W):
-            settle(u, k)
-        add_shard(arrivals[k][0])
-
-    halo = low_rows.shape[1]
+    log_v[...] = jnp.transpose(logs)[0:heads, :]
+    log_copy = pltpu.make_async_copy(log_v, log_out, out_sem.at[0])
+    log_copy.start()
+
+    @pl.when(jnp.logical_not(inner))
+    def _():
+        gate()
+
     reach = conv_taps.shape[0] // 2
-    acc = g_acc[...]
-    gated[...] = (acc[:, 0:cols] * jax.nn.sigmoid(acc[:, cols : 2 * cols])).astype(BF16).reshape(n_fs, rows, cols)
-    up_copy = remote(
-        gated.at[:, pl.ds(rows - halo, halo), :], low_rows, halo_send.at[0], halo_recv.at[0], {"sp": z + 1}
-    )
-    down_copy = remote(
-        gated.at[:, pl.ds(0, halo), :], high_rows, halo_send.at[1], halo_recv.at[1], {"sp": z - 1}
-    )
-
-    @pl.when(z < n_sp - 1)
-    def _():
-        up_copy.start()
-
-    @pl.when(z > 0)
-    def _():
-        down_copy.start()
-
     padded[:, halo : halo + rows, :] = gated[...].astype(F32)
     relay(H, last)
 
@@ -564,8 +584,7 @@
         ref = mixed.at[s, :, pl.ds(pl.multiple_of(head_rows + c * cols, LANES), cols)]
         return remote(ref, ref, conv_send.at[s, i], conv_recv.at[s, i], {"fs": others[i]})
 
-    own_lanes = lanes_at(c, cols)
-    taps = conv_taps[:, own_lanes].astype(F32)
+    taps = conv_taps[...].astype(F32)
     all_gains = row_of(group_gain).astype(F32)
     gains = all_gains[:, 0:cols]
     for i in range(1, n_fs):
@@ -582,8 +601,7 @@
         mixed[s, :, pl.ds(pl.multiple_of(head_rows + c * cols, LANES), cols)] = branch.astype(BF16)
         for i in range(len(others)):
             conv_copy(s, i).start()
-        if s == 1:
-            relay(C, last)
+    relay(C, last)
 
     for i in range(len(others)):
         for h in range(heads):
@@ -592,48 +610,42 @@
         for i in range(len(others)):
             conv_copy(s, i).wait_recv()
 
-    def p_copy(i):
+    def place(core, shard):
+        first = (shard % half_sp) * (n_fs * out_cols) + c * out_cols
+        return placed.at[core, :, pl.ds(pl.multiple_of(first, LANES), out_cols)]
+
+    def fin_copy(shard, j):
+        seq = others[j] if j < len(others) else c
         return remote(
-            parts.at[peer * half_sp + i], peer_parts.at[i], p_send.at[i], p_recv.at[i], {"tp": peer}
+            parts.at[shard, pl.ds(pl.multiple_of(seq * rows, LANES), rows), :], place(t, shard),
+            fin_send.at[shard, j], fin_recv.at[t, shard % half_sp, j], {"fs": seq, "tp": shard // half_sp},
         )
 
-    def fin_copy(i, j):
-        return remote(
-            final.at[i, pl.ds(pl.multiple_of(others[j] * rows, LANES), rows), :],
-            out_v.at[:, pl.ds(pl.multiple_of(i * n_fs * out_cols + c * out_cols, LANES), out_cols)],
-            fin_send.at[i, j], fin_recv.at[i, j], {"fs": others[j]},
+    def add_part(shard, between):
+        part = dot(mixed[:, :, 0:head_rows].reshape(n_fs * rows, head_rows), w_o[shard, 0:head_rows, :])
+        between()
+        part = part + dot(
+            mixed[:, :, head_rows:out_rows].reshape(n_fs * rows, out_rows - head_rows), w_o[shard, head_rows:out_rows, :]
         )
-
-    def add_part(shard):
-        part = dot(mixed[...].reshape(n_fs * rows, out_rows), w_o[shard])
         parts[shard] = part.astype(BF16)
-        for i in range(half_sp):
-            @pl.when(shard == peer * half_sp + i)
-            def _():
-                p_copy(i).start()
-
-    def finish(shard):
-        for i in range(half_sp):
-            @pl.when(shard == t * half_sp + i)
-            def _():
-                p_copy(i).wait_recv()
-                total = parts[t * half_sp + i].astype(F32) + peer_parts[i].astype(F32)
-                final[i] = total.astype(BF16)
-                for j in range(len(others)):
-                    fin_copy(i, j).start()
-                out_v[:, pl.ds(pl.multiple_of(i * n_fs * out_cols + c * out_cols, LANES), out_cols)] = final[
-                    i, pl.ds(pl.multiple_of(c * rows, LANES), rows), :
-                ]
-
-    shards = [z] + [shard for shard, _ in arrivals]
-    for k, shard in enumerate(shards):
-        if k:
-            settle(H, k - 1)
-            settle(C, k - 1)
-        add_part(shard)
-        if k:
-            finish(shards[k - 1])
-    finish(shards[-1])
+        for j in range(len(others)):
+            fin_copy(shard, j).start()
+
+        @pl.when(shard // half_sp != t)
+        def _():
+            fin_copy(shard, len(others)).start()
+
+        @pl.when(shard // half_sp == t)
+        def _():
+            first = (shard % half_sp) * (n_fs * out_cols) + c * out_cols
+            placed[t, :, pl.ds(pl.multiple_of(first, LANES), out_cols)] = parts[
+                shard, pl.ds(pl.multiple_of(c * rows, LANES), rows), :
+            ]
+
+    add_part(z, lambda: None)
+    for k in range(n_sp - 1):
+        settle(H, k)
+        add_part(arrivals[k][0], functools.partial(settle, C, k))
 
     for u in (Q, K, V, W, H, C):
         own(u, lambda copy: copy.wait_send())
@@ -669,11 +681,33 @@
     def _():
         down_copy.wait_send()
 
+    for shard in range(n_sp):
+        for j in range(len(others)):
+            fin_copy(shard, j).wait_send()
+
+        @pl.when(shard // half_sp != t)
+        def _():
+            fin_copy(shard, len(others)).wait_send()
+
+    out_copies = []
     for i in range(half_sp):
-        p_copy(i).wait_send()
         for j in range(len(others)):
-            fin_copy(i, j).wait()
-    out[...] = out_v[...]
+            for core in range(n_tp):
+                remote(
+                    parts.at[0, pl.ds(0, rows), :], place(0, i), fin_send.at[0, j], fin_recv.at[core, i, j], {"tp": peer}
+                ).wait_recv()
+        remote(
+            parts.at[0, pl.ds(0, rows), :], place(0, i), fin_send.at[0, 0], fin_recv.at[peer, i, len(others)], {"tp": peer}
+        ).wait_recv()
+        span = pl.ds(i * n_fs * out_cols, n_fs * out_cols)
+        total = placed[0, :, span].astype(F32) + placed[1, :, span].astype(F32)
+        out_v[:, span] = total.astype(BF16)
+        copy = pltpu.make_async_copy(out_v.at[:, span], out.at[:, span], out_sem.at[1 + i])
+        copy.start()
+        out_copies.append(copy)
+    log_copy.wait()
+    for copy in out_copies:
+        copy.wait()
 
 
 def fused_device(n_sp, n_fs, *args):
@@ -688,18 +722,17 @@
     q_cols = q_rank // n_fs
     halo = (conv_taps.shape[0] // 2 + 15) // 16 * 16
     tables = jnp.asarray(rope_tables(n_sp * rows))
-    vmem = pl.BlockSpec(memory_space=pltpu.VMEM)
     hbm = pl.BlockSpec(memory_space=pltpu.HBM)
     operands = [
-        (tokens, hbm), (norm_gain, vmem), (query_down, hbm), (query_gain, vmem),
-        (latent_down, hbm), (latent_gain, vmem), (rope_down.T, hbm), (query_up, hbm),
-        (key_up, hbm), (value_up, hbm), (glu_value, hbm), (glu_gate, hbm), (conv_taps, vmem),
-        (group_gain, vmem), (head_proj, hbm), (channel_proj, hbm), (tables, hbm),
+        tokens, norm_gain, query_down, query_gain, latent_down, latent_gain, rope_down.T, query_up,
+        key_up, value_up, glu_value, glu_gate, conv_taps, group_gain, head_proj, channel_proj, tables,
     ]
     like = lambda a: pltpu.VMEM(a.shape, a.dtype)
     dma = pltpu.SemaphoreType.DMA
     half_sp = n_sp // 2
     scratch = [
+        like(norm_gain), like(query_gain), like(latent_gain), pltpu.VMEM((conv_taps.shape[0], cols), BF16), like(group_gain),
+        pltpu.VMEM((heads, rows), F32),
         pltpu.VMEM((n_sp, depth, q_cols), BF16),
         pltpu.VMEM((n_sp, depth, 2 * cols), BF16),
         pltpu.VMEM((n_sp, out_rows, out_cols), BF16),
@@ -718,13 +751,12 @@
         pltpu.VMEM((n_fs, rows + 2 * halo, cols), F32),
         pltpu.VMEM((n_fs, rows, out_rows), BF16),
         pltpu.VMEM((n_sp, n_fs * rows, out_cols), BF16),
-        pltpu.VMEM((half_sp, n_fs * rows, out_cols), BF16),
-        pltpu.VMEM((half_sp, n_fs * rows, out_cols), BF16),
+        pltpu.VMEM((2, rows, half_sp * n_fs * out_cols), BF16),
         pltpu.VMEM((rows, half_sp * n_fs * out_cols), BF16),
-        dma((12,)), dma((6, n_sp)), dma((6, n_sp, 3)), dma((2, n_sp)), dma((2, n_sp)),
+        dma((17,)), dma((6, n_sp)), dma((6, n_sp, 3)), dma((2, n_sp)), dma((2, n_sp)),
         dma((3,)), dma((3,)), dma((3,)), dma((3,)), dma((n_fs,)), dma((n_fs // 2, 2)),
         dma((heads, 3)), dma((heads, 3)), dma((2,)), dma((2,)), dma((n_fs, 3)), dma((n_fs, 3)),
-        dma((half_sp,)), dma((half_sp,)), dma((half_sp, 3)), dma((half_sp, 3)),
+        dma((2, half_sp, 4)), dma((n_sp, 4)), dma((1 + half_sp,)),
         pltpu.SemaphoreType.REGULAR,
     ]
     return pl.pallas_call(
@@ -733,14 +765,14 @@
             jax.ShapeDtypeStruct((rows, half_sp * n_fs * out_cols), BF16),
             jax.ShapeDtypeStruct((heads, rows), F32),
         ),
-        in_specs=[spec for _, spec in operands],
-        out_specs=(vmem, vmem),
+        in_specs=[hbm] * len(operands),
+        out_specs=(hbm, hbm),
         scratch_shapes=scratch,
         compiler_params=pltpu.CompilerParams(
             collective_id=0, has_side_effects=True, vmem_limit_bytes=63 * 1024 * 1024
         ),
         name="fused_layer",
-    )(*[value for value, _ in operands])
+    )(*operands)
 
 
 def solution(mesh):

time: 62.5 us -> 57.1 us (0.914)
  Pallas kernels: 59.4 us -> 54.1 us
    pallas_call x1, Pallas kernels: 59.4 us -> 54.1 us  [fused_device(): pl.pallas_call(functools.partial(fused_kernel, n_sp), out_shape=(jax.Shap...]
where the time goes in v2:
time: 57.1 us; the launch traced here: 57 us
  Pallas kernels  54.1 us (95%)
  local copies, waits for them, and re-layouts  2.25 us (4%)
  between operations  0.65 us (1%)
    pallas_call x1, Pallas kernels, fused_device(): pl.pallas_call(functools.partial(fused_kernel, n_sp), out_shape=(jax.Shap...  54.1 us
    unnamed x4, local copies, waits for them, and re-layouts  2.25 us

profile of v2, /device:TPU:1, one launch (start us, length us, event | category | flops | bytes accessed | tf_op | source)
XLA Modules:
  0.0 57.0 jit_solution(7511784159168665241)
XLA Ops:
  0.6 54.1 %fused_layer.1 = (bf16[128,1024]{1,0:T(8,128)(2,1)}, f32[4,128]{1,0:T(4,128)}) custom-call(bf16[128,2048]{1,0:T(8,128)(2,1)} %tokens.1, bf16[2048]{0:T(1024)(128)(2,1)} %norm_gain_in.1, bf16[512,512]{1,0:T(8,128)(2,1)} %query_down.1, bf16[512]{0:T(512)(128)(2,1)} %query_gain_in.1, bf16[2048,256]{1,0:T(8,128)(2,1)} %latent_down.1, ...), custom_call_target="tpu_custom_call" | custom-call | tf_op jit(solution)/shard_map/fused_layer/pallas_call | solution.py:762
  54.7 0.0 copy-start
  54.7 1.7 %copy.21 = bf16[128,1024]{1,0:T(8,128)(2,1)} copy(bf16[128,1024]{1,0:T(8,128)(2,1)} %get-tuple-element.4) | data formatting | bytes 524288
  56.4 0.0 copy-done
  56.4 0.6 %copy.22 = f32[4,128]{1,0:T(4,128)} copy(f32[4,128]{1,0:T(4,128)S(1)} %copy-done) | data formatting | bytes 4096
Async XLA Ops:
  54.7 1.7 %copy-start = (f32[4,128]{1,0:T(4,128)S(1)}, f32[4,128]{1,0:T(4,128)}, u32[]{:S(2)}) copy-start(f32[4,128]{1,0:T(4,128)} %get-tuple-element.5) | copy-start | bytes 6148

commit v3 on v2

--- a/solution.py
+++ b/solution.py
@@ -217,13 +217,14 @@
     n_sp,
     tokens, norm_gain_in, query_down, query_gain_in, latent_down, latent_gain_in, rope_down, query_up,
     key_up, value_up, glu_value, glu_gate, taps_in, group_gain_in, head_proj, channel_proj, tables,
-    out, log_out,
+    placed, log_out,
     norm_gain, query_gain, latent_gain, conv_taps, group_gain, log_v,
     w_q, w_g, w_o, tok_v, lat_v, rope_v, qup_v, kup_v, vup_v, tab_v,
     normed, keys, key_tmp, q_out, q_lat, q_scr, g_acc, gated, low_rows, high_rows, padded,
-    mixed, parts, placed, out_v,
+    mixed, parts, w_full, mixed_o, part_o,
     load_sem, z_recv, z_send, pair_recv, pair_send, n_recv, n_send, np_recv, np_send, q_recv, q_send,
     head_recv, head_send, halo_recv, halo_send, conv_recv, conv_send, fin_recv, fin_send, out_sem,
+    up_recv, up_send, back_recv, back_send,
     corner_sem,
 ):
     z = lax.axis_index("sp")
@@ -286,6 +287,8 @@
     load("lg", latent_gain_in, latent_gain)
     load("taps", taps_in.at[:, lanes_at(c, cols)], conv_taps)
     load("gg", group_gain_in, group_gain)
+    load("hf", head_proj, w_full.at[pl.ds(0, head_rows), :])
+    load("cf", channel_proj, w_full.at[pl.ds(head_rows, out_rows - head_rows), :])
 
     loads["tok"].wait()
     loads["ng"].wait()
@@ -329,11 +332,13 @@
         return remote(ref, ref, z_send.at[u, shard, kind], z_recv.at[u, shard], {"sp": target})
 
     def own(u, action):
-        @pl.when(z > 0)
+        skip = 1 if u in (H, C) else 0
+
+        @pl.when(z > skip)
         def _():
             action(z_copy(u, z, LOW, z - 1))
 
-        @pl.when(z < n_sp - 1)
+        @pl.when(z < n_sp - 1 - skip)
         def _():
             action(z_copy(u, z, HIGH, z + 1))
 
@@ -356,6 +361,19 @@
         shard, target = arrivals[k]
 
         @pl.when(forwards(k))
+        def _():
+            copy = z_copy(u, shard, FWD, target)
+            copy.wait_recv()
+            copy.start()
+
+    inner = (z > 0) & (z < n_sp - 1)
+    lower = 2 * z < n_sp
+    outer = jnp.where(lower, 0, n_sp - 1)
+    near = jnp.where(lower, 1, n_sp - 2)
+    far = jnp.where(lower, n_sp - 2, 1)
+
+    def pass_on(u, shard, target):
+        @pl.when(inner)
         def _():
             copy = z_copy(u, shard, FWD, target)
             copy.wait_recv()
@@ -491,7 +509,6 @@
         def _():
             down_copy.start()
 
-    inner = (z > 0) & (z < n_sp - 1)
     add_shard(z, True)
     relay(W, last)
 
@@ -509,6 +526,8 @@
         def _():
             remote(q_out.at[0], q_lat.at[source], q_send.at[0, 0], q_recv.at[source], {"tp": peer}).wait_recv()
 
+    for u in (H, C):
+        pass_on(u, outer, far)
     whole_q = jnp.concatenate([q_lat[i] for i in range(n_fs)], axis=1)
     latent_query = rms_scale(whole_q, row_of(query_gain)).astype(BF16)
     q_scr[...] = dot(latent_query, qup_v[...])
@@ -543,13 +562,24 @@
     shifted = pltpu.roll(whole, whole.shape[1] - ROPE, 1)
     lane = lax.broadcasted_iota(jnp.int32, (rows, LANES), 1)
     logs = jnp.zeros((rows, LANES), F32)
-    relays = {heads - 1: [(u, k) for u in (H, C) for k in range(last)]}
+
+    def up_copy_of(index, group):
+        ref = mixed.at[c, :, lanes_at(group, cols)]
+        return remote(ref, mixed_o.at[:, lanes_at(group, cols)], up_send.at[index], up_recv.at[index], {"sp": near})
+
+    def send_up(index, group):
+        @pl.when(jnp.logical_not(inner))
+        def _():
+            up_copy_of(index, group).start()
+
     for h in range(heads):
         logs = jnp.where(lane == h, attend(h, shifted), logs)
         for i in range(len(others)):
             head_copy(h, i).start()
-        for u, k in relays.get(h, []):
-            relay(u, k)
+        send_up(h, h)
+        if h == 0:
+            pass_on(H, far, outer)
+    pass_on(C, far, outer)
     log_v[...] = jnp.transpose(logs)[0:heads, :]
     log_copy = pltpu.make_async_copy(log_v, log_out, out_sem.at[0])
     log_copy.start()
@@ -560,7 +590,6 @@
 
     reach = conv_taps.shape[0] // 2
     padded[:, halo : halo + rows, :] = gated[...].astype(F32)
-    relay(H, last)
 
     @pl.when(z > 0)
     def _():
@@ -589,7 +618,9 @@
     gains = all_gains[:, 0:cols]
     for i in range(1, n_fs):
         gains = jnp.where(c == i, all_gains[:, i * cols : (i + 1) * cols], gains)
-    for s in range(n_fs):
+    relay(H, last)
+
+    def conv_seq(s):
         filtered = jnp.zeros((rows, cols), F32)
         for j in range(conv_taps.shape[0]):
             first = halo - reach + j
@@ -599,14 +630,42 @@
         branch = centred * lax.rsqrt(spread + norm_eps) * gains
         branch = branch * jax.nn.sigmoid(branch)
         mixed[s, :, pl.ds(pl.multiple_of(head_rows + c * cols, LANES), cols)] = branch.astype(BF16)
+
+    for i in (2, 0, 1):
+        conv_seq(others[i])
+        conv_copy(others[i], i).start()
+    conv_seq(c)
+    send_up(heads + c, heads + c)
+    for s in others + (c,):
         for i in range(len(others)):
-            conv_copy(s, i).start()
+            if s is not others[i]:
+                conv_copy(s, i).start()
     relay(C, last)
+    for i in range(len(others)):
+        conv_copy(c, i).wait_recv()
+        send_up(heads + others[i], heads + others[i])
+
+    back_lanes = lanes_at(z % half_sp, n_fs * out_cols)
+    back_copy = remote(
+        part_o, placed.at[t, :, back_lanes], back_send.at[0], back_recv.at[t], {"sp": outer, "tp": z // half_sp}
+    )
+    for name in ("hf", "cf"):
+        loads[name].wait()
+
+    def neighbour_part():
+        for i in range(heads + n_fs):
+            up_copy_of(i, i).wait_recv()
+        part_o[...] = dot(mixed_o[...], w_full[...]).astype(BF16)
+        back_copy.start()
+
+    @pl.when(inner)
+    def _():
+        neighbour_part()
 
     for i in range(len(others)):
         for h in range(heads):
             head_copy(h, i).wait_recv()
-    for s in range(n_fs):
+    for s in others:
         for i in range(len(others)):
             conv_copy(s, i).wait_recv()
 
@@ -620,6 +679,10 @@
             parts.at[shard, pl.ds(pl.multiple_of(seq * rows, LANES), rows), :], place(t, shard),
             fin_send.at[shard, j], fin_recv.at[t, shard % half_sp, j], {"fs": seq, "tp": shard // half_sp},
         )
+
+    def keep_copy(shard):
+        ref = parts.at[shard, pl.ds(pl.multiple_of(c * rows, LANES), rows), :]
+        return pltpu.make_async_copy(ref, place(t, shard), out_sem.at[1 + shard % half_sp])
 
     def add_part(shard, between):
         part = dot(mixed[:, :, 0:head_rows].reshape(n_fs * rows, head_rows), w_o[shard, 0:head_rows, :])
@@ -637,13 +700,15 @@
 
         @pl.when(shard // half_sp == t)
         def _():
-            first = (shard % half_sp) * (n_fs * out_cols) + c * out_cols
-            placed[t, :, pl.ds(pl.multiple_of(first, LANES), out_cols)] = parts[
-                shard, pl.ds(pl.multiple_of(c * rows, LANES), rows), :
-            ]
+            keep_copy(shard).start()
 
     add_part(z, lambda: None)
-    for k in range(n_sp - 1):
+
+    @pl.when(inner)
+    def _():
+        add_part(arrivals[0][0], lambda: None)
+
+    for k in range(1, n_sp - 1):
         settle(H, k)
         add_part(arrivals[k][0], functools.partial(settle, C, k))
 
@@ -681,33 +746,56 @@
     def _():
         down_copy.wait_send()
 
+    for index in range(heads + n_fs):
+        @pl.when(jnp.logical_not(inner))
+        def _():
+            up_copy_of(index, index).wait_send()
+
+    @pl.when(inner)
+    def _():
+        back_copy.wait_send()
+
     for shard in range(n_sp):
-        for j in range(len(others)):
-            fin_copy(shard, j).wait_send()
-
-        @pl.when(shard // half_sp != t)
+        computed = inner | (shard != near)
+
+        @pl.when(computed)
+        def _():
+            for j in range(len(others)):
+                fin_copy(shard, j).wait_send()
+
+        @pl.when(computed & (shard // half_sp != t))
         def _():
             fin_copy(shard, len(others)).wait_send()
 
-    out_copies = []
     for i in range(half_sp):
-        for j in range(len(others)):
+        shard = t * half_sp + i
+        computed = inner | (shard != near)
+
+        def arrived(core, j):
+            remote(
+                parts.at[0, pl.ds(0, rows), :], place(0, i), fin_send.at[0, j], fin_recv.at[core, i, j], {"tp": peer}
+            ).wait_recv()
+
+        @pl.when(computed)
+        def _():
+            for core in range(n_tp):
+                for j in range(len(others)):
+                    arrived(core, j)
+            arrived(peer, len(others))
+            keep_copy(shard).wait()
+
+        @pl.when(jnp.logical_not(computed))
+        def _():
             for core in range(n_tp):
                 remote(
-                    parts.at[0, pl.ds(0, rows), :], place(0, i), fin_send.at[0, j], fin_recv.at[core, i, j], {"tp": peer}
+                    part_o, placed.at[0, :, lanes_at(i, n_fs * out_cols)], back_send.at[0], back_recv.at[core], {"tp": peer}
                 ).wait_recv()
-        remote(
-            parts.at[0, pl.ds(0, rows), :], place(0, i), fin_send.at[0, 0], fin_recv.at[peer, i, len(others)], {"tp": peer}
-        ).wait_recv()
-        span = pl.ds(i * n_fs * out_cols, n_fs * out_cols)
-        total = placed[0, :, span].astype(F32) + placed[1, :, span].astype(F32)
-        out_v[:, span] = total.astype(BF16)
-        copy = pltpu.make_async_copy(out_v.at[:, span], out.at[:, span], out_sem.at[1 + i])
-        copy.start()
-        out_copies.append(copy)
     log_copy.wait()
-    for copy in out_copies:
-        copy.wait()
+
+
+def finish_kernel(placed, log_in, out, log_out):
+    out[...] = (placed[0].astype(F32) + placed[1].astype(F32)).astype(BF16)
+    log_out[...] = log_in[...]
 
 
 def fused_device(n_sp, n_fs, *args):
@@ -751,20 +839,23 @@
         pltpu.VMEM((n_fs, rows + 2 * halo, cols), F32),
         pltpu.VMEM((n_fs, rows, out_rows), BF16),
         pltpu.VMEM((n_sp, n_fs * rows, out_cols), BF16),
-        pltpu.VMEM((2, rows, half_sp * n_fs * out_cols), BF16),
-        pltpu.VMEM((rows, half_sp * n_fs * out_cols), BF16),
-        dma((17,)), dma((6, n_sp)), dma((6, n_sp, 3)), dma((2, n_sp)), dma((2, n_sp)),
+        pltpu.VMEM((out_rows, n_fs * out_cols), BF16),
+        pltpu.VMEM((rows, out_rows), BF16),
+        pltpu.VMEM((rows, n_fs * out_cols), BF16),
+        dma((19,)), dma((6, n_sp)), dma((6, n_sp, 3)), dma((2, n_sp)), dma((2, n_sp)),
         dma((3,)), dma((3,)), dma((3,)), dma((3,)), dma((n_fs,)), dma((n_fs // 2, 2)),
         dma((heads, 3)), dma((heads, 3)), dma((2,)), dma((2,)), dma((n_fs, 3)), dma((n_fs, 3)),
         dma((2, half_sp, 4)), dma((n_sp, 4)), dma((1 + half_sp,)),
+        dma((heads + n_fs,)), dma((heads + n_fs,)), dma((2,)), dma((1,)),
         pltpu.SemaphoreType.REGULAR,
     ]
-    return pl.pallas_call(
+    shapes = (
+        jax.ShapeDtypeStruct((rows, half_sp * n_fs * out_cols), BF16),
+        jax.ShapeDtypeStruct((heads, rows), F32),
+    )
+    placed, logs = pl.pallas_call(
         functools.partial(fused_kernel, n_sp),
-        out_shape=(
-            jax.ShapeDtypeStruct((rows, half_sp * n_fs * out_cols), BF16),
-            jax.ShapeDtypeStruct((heads, rows), F32),
-        ),
+        out_shape=(jax.ShapeDtypeStruct((2,) + shapes[0].shape, BF16), shapes[1]),
         in_specs=[hbm] * len(operands),
         out_specs=(hbm, hbm),
         scratch_shapes=scratch,
@@ -773,6 +864,7 @@
         ),
         name="fused_layer",
     )(*operands)
+    return pl.pallas_call(finish_kernel, out_shape=shapes, name="finish")(placed, logs)
 
 
 def solution(mesh):

time: 57.1 us -> 53.5 us (0.937)
  the two profiles are of different devices: /device:TPU:1 before, /device:TPU:16 now
where the time goes in v3:
time: 53.5 us; the launch traced here: 53.4 us
  Pallas kernels  52.7 us (99%)
  between operations  0.64 us (1%)
    pallas_call x1, Pallas kernels, fused_device(): pl.pallas_call(functools.partial(fused_kernel, n_sp), out_shape=(jax.Shap...  50.9 us
    pallas_call x1, Pallas kernels, fused_device(): pl.pallas_call(finish_kernel, out_shape=shapes, name='finish')(placed, logs)  1.81 us

profile of v3, /device:TPU:16, one launch (start us, length us, event | category | flops | bytes accessed | tf_op | source)
XLA Modules:
  0.0 53.4 jit_solution(7297987472186945047)
XLA Ops:
  0.6 50.9 %fused_layer.1 = (bf16[2,128,1024]{2,1,0:T(8,128)(2,1)}, f32[4,128]{1,0:T(4,128)}) custom-call(bf16[128,2048]{1,0:T(8,128)(2,1)} %tokens.1, bf16[2048]{0:T(1024)(128)(2,1)} %norm_gain_in.1, bf16[512,512]{1,0:T(8,128)(2,1)} %query_down.1, bf16[512]{0:T(512)(128)(2,1)} %query_gain_in.1, bf16[2048,256]{1,0:T(8,128)(2,1)} %latent_down.1, ...), custom_call_target="tpu_custom_call" | custom-call | tf_op jit(solution)/shard_map/fused_layer/pallas_call | solution.py:856
  51.6 1.8 %finish.1 = (bf16[128,1024]{1,0:T(8,128)(2,1)}, f32[4,128]{1,0:T(4,128)}) custom-call(bf16[2,128,1024]{2,1,0:T(8,128)(2,1)} %get-tuple-element.4.placed, f32[4,128]{1,0:T(4,128)} %get-tuple-element.5.log_in), custom_call_target="tpu_custom_call" | custom-call | tf_op jit(solution)/shard_map/finish/pallas_call | solution.py:867

commit v4 on v3

--- a/solution.py
+++ b/solution.py
@@ -180,8 +180,9 @@
 MESH = pl.DeviceIdType.MESH
 F32 = jnp.float32
 BF16 = jnp.bfloat16
-LOW, HIGH, FWD = range(3)
-Q, K, V, W, H, C = range(6)
+Q, K, H, C, G = range(5)
+PIECES = 4
+RING = 32
 
 
 def rope_tables(length):
@@ -222,10 +223,8 @@
     w_q, w_g, w_o, tok_v, lat_v, rope_v, qup_v, kup_v, vup_v, tab_v,
     normed, keys, key_tmp, q_out, q_lat, q_scr, g_acc, gated, low_rows, high_rows, padded,
     mixed, parts, w_full, mixed_o, part_o,
-    load_sem, z_recv, z_send, pair_recv, pair_send, n_recv, n_send, np_recv, np_send, q_recv, q_send,
-    head_recv, head_send, halo_recv, halo_send, conv_recv, conv_send, fin_recv, fin_send, out_sem,
-    up_recv, up_send, back_recv, back_send,
-    corner_sem,
+    load_sem, ring_sem, z_recv, pair_recv, n_recv, np_recv, q_recv, head_recv, halo_recv, halo_send,
+    conv_recv, fin_recv, out_sem, up_recv, back_recv, back_send, nr_recv, hr_recv, cr_recv, corner_recv,
 ):
     z = lax.axis_index("sp")
     c = lax.axis_index("fs")
@@ -265,30 +264,32 @@
 
     loads = {}
 
-    def load(name, src, dst):
-        copy = pltpu.make_async_copy(src, dst, load_sem.at[len(loads)])
+    def load(name, slot, src, dst):
+        copy = pltpu.make_async_copy(src, dst, load_sem.at[slot])
         copy.start()
         loads[name] = copy
 
-    load("tok", tokens, tok_v)
-    load("ng", norm_gain_in, norm_gain)
-    load("wq", query_down.at[:, lanes_at(c, q_cols)], w_q.at[z])
-    load("wv", glu_value.at[:, lanes_at(c, cols)], w_g.at[z, :, pl.ds(0, cols)])
-    load("wt", glu_gate.at[:, lanes_at(c, cols)], w_g.at[z, :, pl.ds(cols, cols)])
-    load("lat", latent_down, lat_v)
-    load("rope", rope_down, rope_v)
-    load("tab", tables.at[:, pl.ds(pl.multiple_of(z * rows, LANES), rows), :], tab_v)
-    load("hp", head_proj.at[:, lanes_at(c, out_cols)], w_o.at[z, pl.ds(0, head_rows), :])
-    load("cp", channel_proj.at[:, lanes_at(c, out_cols)], w_o.at[z, pl.ds(head_rows, out_rows - head_rows), :])
-    load("qup", query_up, qup_v)
-    load("kup", key_up, kup_v)
-    load("vup", value_up, vup_v)
-    load("qg", query_gain_in, query_gain)
-    load("lg", latent_gain_in, latent_gain)
-    load("taps", taps_in.at[:, lanes_at(c, cols)], conv_taps)
-    load("gg", group_gain_in, group_gain)
-    load("hf", head_proj, w_full.at[pl.ds(0, head_rows), :])
-    load("cf", channel_proj, w_full.at[pl.ds(head_rows, out_rows - head_rows), :])
+    load("tok", 0, tokens, tok_v)
+    load("ng", 1, norm_gain_in, norm_gain)
+    load("wq", 2, query_down.at[:, lanes_at(c, q_cols)], w_q.at[z])
+    load("wv", 3, glu_value.at[:, lanes_at(c, cols)], w_g.at[z, :, pl.ds(0, cols)])
+    load("wt", 4, glu_gate.at[:, lanes_at(c, cols)], w_g.at[z, :, pl.ds(cols, cols)])
+    load("lat", 5, latent_down, lat_v)
+    load("rope", 6, rope_down, rope_v)
+    load("tab", 7, tables.at[:, pl.ds(pl.multiple_of(z * rows, LANES), rows), :], tab_v)
+    load("lg", 8, latent_gain_in, latent_gain)
+
+    def load_rest():
+        load("hp", 0, head_proj.at[:, lanes_at(c, out_cols)], w_o.at[z, pl.ds(0, head_rows), :])
+        load("cp", 1, channel_proj.at[:, lanes_at(c, out_cols)], w_o.at[z, pl.ds(head_rows, out_rows - head_rows), :])
+        load("qup", 2, query_up, qup_v)
+        load("kup", 3, key_up, kup_v)
+        load("vup", 4, value_up, vup_v)
+        load("qg", 5, query_gain_in, query_gain)
+        load("taps", 6, taps_in.at[:, lanes_at(c, cols)], conv_taps)
+        load("gg", 7, group_gain_in, group_gain)
+        load("hf", 8, head_proj, w_full.at[pl.ds(0, head_rows), :])
+        load("cf", 9, channel_proj, w_full.at[pl.ds(head_rows, out_rows - head_rows), :])
 
     loads["tok"].wait()
     loads["ng"].wait()
@@ -299,17 +300,52 @@
 
     ends = (z == 0).astype(jnp.int32) + (z == n_sp - 1).astype(jnp.int32)
     pl.semaphore_wait(barrier, len(sides) + 2 - ends)
-    pl.semaphore_signal(corner_sem, inc=1, device_id={"fs": c_x}, device_id_type=MESH)
-
-    def remote(src, dst, send_sem, recv_sem, device):
-        return pltpu.make_async_remote_copy(
-            src_ref=src, dst_ref=dst, send_sem=send_sem, recv_sem=recv_sem,
-            device_id=device, device_id_type=MESH,
-        )
+
+    sent = []
+
+    def when(cond, action):
+        if cond is None:
+            action()
+        else:
+            pl.when(cond)(action)
+
+    def both(first, second):
+        return second if first is None else first & second
+
+    def remote(src, dst, recv_sem, device):
+        def make(send_sem):
+            return pltpu.make_async_remote_copy(
+                src_ref=src, dst_ref=dst, send_sem=send_sem, recv_sem=recv_sem,
+                device_id=device, device_id_type=MESH,
+            )
+
+        return make
+
+    def drain(entry):
+        copy, cond = entry
+        when(cond, copy.wait_send)
+
+    def send(make, cond=None):
+        slot = len(sent) % RING
+        if len(sent) >= RING:
+            drain(sent[-RING])
+        copy = make(ring_sem.at[slot])
+        when(cond, copy.start)
+        sent.append((copy, cond))
+
+    def arrive(make):
+        make(ring_sem.at[0]).wait_recv()
 
     q_half = depth // n_tp
-    g_half = depth // 2
+    piece = depth // PIECES
     k_half = rows // n_tp
+    inner = (z > 0) & (z < n_sp - 1)
+    at_end = jnp.logical_not(inner)
+    lower = 2 * z < n_sp
+    outer = jnp.where(lower, 0, n_sp - 1)
+    near = jnp.where(lower, 1, n_sp - 2)
+    far = jnp.where(lower, n_sp - 2, 1)
+    neighbour = jnp.where(lower, z + 1, z - 1)
 
     def half(first, size):
         return pl.ds(pl.multiple_of(first * size, 16), size)
@@ -319,95 +355,87 @@
             return w_q.at[shard, half(side, q_half), :]
         if u == K:
             return keys.at[shard, half(side, k_half), :]
-        if u == V:
-            return w_g.at[shard, pl.ds(0, g_half), :]
-        if u == W:
-            return w_g.at[shard, pl.ds(g_half, depth - g_half), :]
         if u == H:
             return w_o.at[shard, pl.ds(0, head_rows), :]
-        return w_o.at[shard, pl.ds(head_rows, out_rows - head_rows), :]
-
-    def z_copy(u, shard, kind, target):
+        if u == C:
+            return w_o.at[shard, pl.ds(head_rows, out_rows - head_rows), :]
+        return w_g.at[shard, pl.ds((u - G) * piece, piece), :]
+
+    def slot_of(shard, at):
+        return shard - (shard > at).astype(jnp.int32)
+
+    def z_copy(u, shard, target):
         ref = block(u, shard)
-        return remote(ref, ref, z_send.at[u, shard, kind], z_recv.at[u, shard], {"sp": target})
-
-    def own(u, action):
+        return remote(ref, ref, z_recv.at[u, slot_of(shard, target)], {"sp": target})
+
+    def z_arrive(u, shard):
+        ref = block(u, shard)
+        arrive(remote(ref, ref, z_recv.at[u, slot_of(shard, z)], {"sp": neighbour}))
+
+    def send_own(u, cond=None):
         skip = 1 if u in (H, C) else 0
-
-        @pl.when(z > skip)
-        def _():
-            action(z_copy(u, z, LOW, z - 1))
-
-        @pl.when(z < n_sp - 1 - skip)
-        def _():
-            action(z_copy(u, z, HIGH, z + 1))
-
-    def send_own(u):
-        own(u, lambda copy: copy.start())
+        send(z_copy(u, z, z - 1), both(cond, z > skip))
+        send(z_copy(u, z, z + 1), both(cond, z < n_sp - 1 - skip))
 
     nearest = jnp.minimum(z, n_sp - 1 - z)
     arrivals = []
     for k in range(n_sp - 1):
-        both = k < 2 * nearest
-        distance = jnp.where(both, k // 2 + 1, k - nearest + 1)
-        from_low = jnp.where(both, 1 - k % 2, (2 * z > n_sp - 1).astype(jnp.int32))
+        two_sided = k < 2 * nearest
+        distance = jnp.where(two_sided, k // 2 + 1, k - nearest + 1)
+        from_low = jnp.where(two_sided, 1 - k % 2, (2 * z > n_sp - 1).astype(jnp.int32))
         arrivals.append((z - distance * (2 * from_low - 1), z + 2 * from_low - 1))
 
-    def forwards(k):
-        target = arrivals[k][1]
-        return (target >= 0) & (target < n_sp)
+    def pass_on(u, shard, target):
+        when(inner, lambda: z_arrive(u, shard))
+        send(z_copy(u, shard, target), inner)
 
     def relay(u, k):
-        shard, target = arrivals[k]
-
-        @pl.when(forwards(k))
-        def _():
-            copy = z_copy(u, shard, FWD, target)
-            copy.wait_recv()
-            copy.start()
-
-    inner = (z > 0) & (z < n_sp - 1)
-    lower = 2 * z < n_sp
-    outer = jnp.where(lower, 0, n_sp - 1)
-    near = jnp.where(lower, 1, n_sp - 2)
-    far = jnp.where(lower, n_sp - 2, 1)
-
-    def pass_on(u, shard, target):
-        @pl.when(inner)
-        def _():
-            copy = z_copy(u, shard, FWD, target)
-            copy.wait_recv()
-            copy.start()
+        pass_on(u, *arrivals[k])
 
     def settle(u, k):
-        @pl.when(jnp.logical_not(forwards(k)))
-        def _():
-            z_copy(u, arrivals[k][0], FWD, jnp.where(z > 0, z - 1, z + 1)).wait_recv()
+        when(at_end, lambda: z_arrive(u, arrivals[k][0]))
 
     def pair(u, shard, side):
         ref = block(u, shard, side)
-        return remote(ref, ref, pair_send.at[u, shard], pair_recv.at[u, shard], {"tp": peer})
+        return remote(ref, ref, pair_recv.at[u, slot_of(shard, z)], {"tp": peer})
 
     def share(u, k):
         settle(u, k)
-        pair(u, arrivals[k][0], t).start()
-
-    def n_copy(i):
-        ref = normed.at[c, :, lanes_at(t, half_width)]
-        return remote(ref, ref, n_send.at[i], n_recv.at[i], {"fs": others[i]})
+        send(pair(u, arrivals[k][0], t))
+
+    quarter_width = half_width // 2
+
+    def n_block(owner, part):
+        return normed.at[owner, :, lanes_at(2 * t + part, quarter_width)]
+
+    def n_copy(i, part):
+        ref = n_block(c, part)
+        return remote(ref, ref, n_recv.at[i, part], {"fs": others[i]})
+
+    def n_relay(i):
+        ref = n_block(others[i], i)
+        return remote(ref, ref, nr_recv.at[i], {"fs": others[1 - i]})
 
     def n_pair(i, side):
         ref = normed.at[others[i], :, lanes_at(side, half_width)]
-        return remote(ref, ref, np_send.at[i], np_recv.at[i], {"tp": peer})
+        return remote(ref, ref, np_recv.at[i], {"tp": peer})
+
+    def pass_normed(i):
+        arrive(n_copy(i, i))
+        send(n_relay(i))
 
     def share_normed(i):
-        n_copy(i).wait_recv()
-        n_pair(i, t).start()
+        if i < 2:
+            arrive(n_copy(i, 1 - i))
+        else:
+            for j in range(2):
+                arrive(n_relay(j))
+        send(n_pair(i, t))
 
     send_own(Q)
-    send_own(V)
-    n_copy(0).start()
-    n_copy(1).start()
+    for part in range(2):
+        send(n_copy(0, part))
+        send(n_copy(1, 1 - part))
 
     def rotate_lanes(v):
         step = ROPE // 2
@@ -426,59 +454,57 @@
     key_tmp[:, 0:ROPE] = dot_nt(own_normed, rope_v[...])
     keys[z, :, KVR : KVR + LANES] = rotate_lanes(key_tmp[...]).astype(BF16)
     send_own(K)
-
-    pl.semaphore_wait(corner_sem, 1)
-    n_copy(2).start()
+    send_own(G)
+    load_rest()
 
     last = n_sp - 2
     for k in range(last):
         relay(Q, k)
-    send_own(W)
+    send_own(G + 1)
+    pass_normed(0)
+    pass_normed(1)
     for k in range(last):
         relay(K, k)
     share(Q, 0)
     relay(Q, last)
+    for p in range(2, PIECES):
+        send_own(G + p)
+    for k in range(last):
+        relay(G, k)
+    share_normed(0)
+    share_normed(1)
     relay(K, last)
     for k in range(last):
-        relay(V, k)
-    share_normed(0)
-    share_normed(1)
-    share(K, 0)
+        relay(G + 1, k)
     for k in range(1, last):
         share(Q, k)
-        share(K, k)
-    for k in range(last):
-        relay(W, k)
+    share_normed(2)
     share(Q, last)
-    share_normed(2)
-    share(K, last)
-    relay(V, last)
+    for p in range(2, PIECES):
+        for k in range(last):
+            relay(G + p, k)
 
     for i in range(len(others)):
-        n_pair(i, peer).wait_recv()
+        arrive(n_pair(i, peer))
     for k in range(n_sp - 1):
-        pair(Q, arrivals[k][0], peer).wait_recv()
+        arrive(pair(Q, arrivals[k][0], peer))
     seqs = normed[pl.ds(per_core * t, per_core)].reshape(per_core * rows, width)
     q_out[...] = dot(seqs, w_q[...].reshape(n_sp * depth, q_cols)).reshape(per_core, rows, q_cols)
 
-    def q_copies(i):
+    for i in range(per_core):
         seq = per_core * t + i
-        return seq, [
-            remote(q_out.at[i], q_lat.at[c], q_send.at[i, j], q_recv.at[c], {"fs": seq, "tp": core})
-            for j, core in enumerate((t, peer))
-        ]
-
-    for i in range(per_core):
-        seq, (same, other) = q_copies(i)
-        other.start()
-
-        @pl.when(seq != c)
-        def _():
-            same.start()
+        for core in (peer, t):
+            copy = remote(q_out.at[i], q_lat.at[c], q_recv.at[c], {"fs": seq, "tp": core})
+            send(copy, None if core is peer else seq != c)
 
         @pl.when(seq == c)
         def _():
             q_lat[c] = q_out[i]
+
+    for name in ("hp", "cp"):
+        loads[name].wait()
+    for u in (H, C):
+        send_own(u, at_end)
 
     def add_shard(shard, first=False):
         rows_in = normed[:, :, lanes_at(shard, depth)].reshape(n_fs * rows, depth)
@@ -487,16 +513,16 @@
 
     halo = low_rows.shape[1]
     up_copy = remote(
-        gated.at[:, pl.ds(rows - halo, halo), :], low_rows, halo_send.at[0], halo_recv.at[0], {"sp": z + 1}
-    )
+        gated.at[:, pl.ds(rows - halo, halo), :], low_rows, halo_recv.at[0], {"sp": z + 1}
+    )(halo_send.at[0])
     down_copy = remote(
-        gated.at[:, pl.ds(0, halo), :], high_rows, halo_send.at[1], halo_recv.at[1], {"sp": z - 1}
-    )
+        gated.at[:, pl.ds(0, halo), :], high_rows, halo_recv.at[1], {"sp": z - 1}
+    )(halo_send.at[1])
 
     def gate():
         for k in range(n_sp - 1):
-            for u in (V, W):
-                settle(u, k)
+            for p in range(PIECES):
+                settle(G + p, k)
             add_shard(arrivals[k][0])
         acc = g_acc[...]
         gated[...] = (acc[:, 0:cols] * jax.nn.sigmoid(acc[:, cols : 2 * cols])).astype(BF16).reshape(n_fs, rows, cols)
@@ -509,30 +535,35 @@
         def _():
             down_copy.start()
 
+    for p in range(2):
+        relay(G + p, last)
+    for k in range(last):
+        share(K, k)
     add_shard(z, True)
-    relay(W, last)
+    for p in range(2, PIECES):
+        relay(G + p, last)
+    share(K, last)
 
     @pl.when(inner)
     def _():
         gate()
 
-    for name in ("hp", "cp", "qup", "kup", "vup", "qg", "taps", "gg"):
+    for u in (H, C):
+        send_own(u, inner)
+    for name in ("qup", "kup", "vup", "qg", "taps", "gg"):
         loads[name].wait()
-    send_own(H)
-    send_own(C)
 
     for source in range(n_fs):
         @pl.when((c != source) | (t != c // per_core))
         def _():
-            remote(q_out.at[0], q_lat.at[source], q_send.at[0, 0], q_recv.at[source], {"tp": peer}).wait_recv()
-
-    for u in (H, C):
-        pass_on(u, outer, far)
+            arrive(remote(q_out.at[0], q_lat.at[source], q_recv.at[source], {"tp": peer}))
+
+    pass_on(H, outer, far)
     whole_q = jnp.concatenate([q_lat[i] for i in range(n_fs)], axis=1)
     latent_query = rms_scale(whole_q, row_of(query_gain)).astype(BF16)
     q_scr[...] = dot(latent_query, qup_v[...])
     for k in range(n_sp - 1):
-        pair(K, arrivals[k][0], peer).wait_recv()
+        arrive(pair(K, arrivals[k][0], peer))
 
     def attend(h, shifted):
         start = h * (NOPE + ROPE)
@@ -556,35 +587,43 @@
 
     def head_copy(h, i):
         ref = mixed.at[c, :, pl.ds(h * VDIM, VDIM)]
-        return remote(ref, ref, head_send.at[h, i], head_recv.at[h, i], {"fs": others[i]})
+        return remote(ref, ref, head_recv.at[h, i], {"fs": others[i]})
+
+    def head_relay(h):
+        i = h * 2 // heads
+        ref = mixed.at[others[i], :, pl.ds(h * VDIM, VDIM)]
+        return i, remote(ref, ref, hr_recv.at[h], {"fs": others[1 - i]})
+
+    def pass_head(h):
+        i, copy = head_relay(h)
+        arrive(head_copy(h, i))
+        send(copy)
 
     whole = q_scr[...]
     shifted = pltpu.roll(whole, whole.shape[1] - ROPE, 1)
     lane = lax.broadcasted_iota(jnp.int32, (rows, LANES), 1)
     logs = jnp.zeros((rows, LANES), F32)
 
-    def up_copy_of(index, group):
+    def to_near(group):
         ref = mixed.at[c, :, lanes_at(group, cols)]
-        return remote(ref, mixed_o.at[:, lanes_at(group, cols)], up_send.at[index], up_recv.at[index], {"sp": near})
-
-    def send_up(index, group):
-        @pl.when(jnp.logical_not(inner))
-        def _():
-            up_copy_of(index, group).start()
+        return remote(ref, mixed_o.at[:, lanes_at(group, cols)], up_recv.at[group], {"sp": near})
 
     for h in range(heads):
         logs = jnp.where(lane == h, attend(h, shifted), logs)
-        for i in range(len(others)):
-            head_copy(h, i).start()
-        send_up(h, h)
+        for i in range(2):
+            send(head_copy(h, i))
+        send(to_near(h), at_end)
         if h == 0:
-            pass_on(H, far, outer)
-    pass_on(C, far, outer)
+            pass_on(C, outer, far)
     log_v[...] = jnp.transpose(logs)[0:heads, :]
     log_copy = pltpu.make_async_copy(log_v, log_out, out_sem.at[0])
     log_copy.start()
-
-    @pl.when(jnp.logical_not(inner))
+    pass_on(H, far, outer)
+    for h in range(heads):
+        pass_head(h)
+    pass_on(C, far, outer)
+
+    @pl.when(at_end)
     def _():
         gate()
 
@@ -609,9 +648,24 @@
     def _():
         padded[:, halo + rows : 2 * halo + rows, :] = jnp.zeros((n_fs, halo, cols), F32)
 
+    def conv_ref(s, group):
+        return mixed.at[s, :, pl.ds(pl.multiple_of(head_rows + group * cols, LANES), cols)]
+
     def conv_copy(s, i):
-        ref = mixed.at[s, :, pl.ds(pl.multiple_of(head_rows + c * cols, LANES), cols)]
-        return remote(ref, ref, conv_send.at[s, i], conv_recv.at[s, i], {"fs": others[i]})
+        ref = conv_ref(s, c)
+        return remote(ref, ref, conv_recv.at[s, i], {"fs": others[i]})
+
+    def conv_corner():
+        ref = conv_ref(c_d, c)
+        return remote(ref, ref, corner_recv.at[0], {"fs": c_d})
+
+    def conv_corner_in():
+        ref = conv_ref(c, c_d)
+        return remote(ref, ref, corner_recv.at[0], {"fs": c_d})
+
+    def conv_relay(s, i):
+        ref = conv_ref(s, others[i])
+        return remote(ref, ref, cr_recv.at[s], {"fs": others[1 - i]})
 
     taps = conv_taps[...].astype(F32)
     all_gains = row_of(group_gain).astype(F32)
@@ -631,30 +685,38 @@
         branch = branch * jax.nn.sigmoid(branch)
         mixed[s, :, pl.ds(pl.multiple_of(head_rows + c * cols, LANES), cols)] = branch.astype(BF16)
 
-    for i in (2, 0, 1):
-        conv_seq(others[i])
-        conv_copy(others[i], i).start()
+    conv_seq(c_d)
+    send(conv_corner())
+    conv_seq(c_x)
+    send(conv_copy(c_x, 0))
+    conv_seq(c_y)
+    send(conv_copy(c_y, 1))
     conv_seq(c)
-    send_up(heads + c, heads + c)
-    for s in others + (c,):
-        for i in range(len(others)):
-            if s is not others[i]:
-                conv_copy(s, i).start()
+    send(to_near(heads + c), at_end)
+    for s, i in ((c, 0), (c_d, 1), (c_y, 0), (c, 1), (c_d, 0), (c_x, 1)):
+        send(conv_copy(s, i))
+    arrive(conv_copy(c, 0))
+    send(to_near(heads + c_x), at_end)
+    arrive(conv_copy(c, 1))
+    send(to_near(heads + c_y), at_end)
+    send(conv_relay(c, 1))
+    arrive(conv_corner_in())
+    send(to_near(heads + c_d), at_end)
     relay(C, last)
-    for i in range(len(others)):
-        conv_copy(c, i).wait_recv()
-        send_up(heads + others[i], heads + others[i])
+    for s, i in ((c_x, 0), (c_d, 1)):
+        arrive(conv_copy(s, i))
+        send(conv_relay(s, i))
 
     back_lanes = lanes_at(z % half_sp, n_fs * out_cols)
     back_copy = remote(
-        part_o, placed.at[t, :, back_lanes], back_send.at[0], back_recv.at[t], {"sp": outer, "tp": z // half_sp}
-    )
+        part_o, placed.at[t, :, back_lanes], back_recv.at[t], {"sp": outer, "tp": z // half_sp}
+    )(back_send.at[0])
     for name in ("hf", "cf"):
         loads[name].wait()
 
     def neighbour_part():
         for i in range(heads + n_fs):
-            up_copy_of(i, i).wait_recv()
+            arrive(to_near(i))
         part_o[...] = dot(mixed_o[...], w_full[...]).astype(BF16)
         back_copy.start()
 
@@ -662,12 +724,13 @@
     def _():
         neighbour_part()
 
-    for i in range(len(others)):
-        for h in range(heads):
-            head_copy(h, i).wait_recv()
+    for h in range(heads):
+        arrive(head_copy(h, 1 - head_relay(h)[0]))
+        arrive(head_relay(h)[1])
+    for s, i in ((c_y, 1), (c_d, 0), (c_x, 1), (c_y, 0)):
+        arrive(conv_copy(s, i))
     for s in others:
-        for i in range(len(others)):
-            conv_copy(s, i).wait_recv()
+        arrive(conv_relay(s, 0))
 
     def place(core, shard):
         first = (shard % half_sp) * (n_fs * out_cols) + c * out_cols
@@ -677,66 +740,37 @@
         seq = others[j] if j < len(others) else c
         return remote(
             parts.at[shard, pl.ds(pl.multiple_of(seq * rows, LANES), rows), :], place(t, shard),
-            fin_send.at[shard, j], fin_recv.at[t, shard % half_sp, j], {"fs": seq, "tp": shard // half_sp},
+            fin_recv.at[t, shard % half_sp, j], {"fs": seq, "tp": shard // half_sp},
         )
 
     def keep_copy(shard):
         ref = parts.at[shard, pl.ds(pl.multiple_of(c * rows, LANES), rows), :]
         return pltpu.make_async_copy(ref, place(t, shard), out_sem.at[1 + shard % half_sp])
 
-    def add_part(shard, between):
-        part = dot(mixed[:, :, 0:head_rows].reshape(n_fs * rows, head_rows), w_o[shard, 0:head_rows, :])
-        between()
-        part = part + dot(
-            mixed[:, :, head_rows:out_rows].reshape(n_fs * rows, out_rows - head_rows), w_o[shard, head_rows:out_rows, :]
-        )
-        parts[shard] = part.astype(BF16)
-        for j in range(len(others)):
-            fin_copy(shard, j).start()
-
-        @pl.when(shard // half_sp != t)
-        def _():
-            fin_copy(shard, len(others)).start()
-
-        @pl.when(shard // half_sp == t)
-        def _():
-            keep_copy(shard).start()
+    def add_part(shard, between, cond=None):
+        def compute():
+            part = dot(mixed[:, :, 0:head_rows].reshape(n_fs * rows, head_rows), w_o[shard, 0:head_rows, :])
+            between()
+            part = part + dot(
+                mixed[:, :, head_rows:out_rows].reshape(n_fs * rows, out_rows - head_rows), w_o[shard, head_rows:out_rows, :]
+            )
+            parts[shard] = part.astype(BF16)
+
+        when(cond, compute)
+        for j in (2, 0, 1):
+            send(fin_copy(shard, j), cond)
+        mine = shard // half_sp == t
+        send(fin_copy(shard, len(others)), both(cond, jnp.logical_not(mine)))
+        when(both(cond, mine), lambda: keep_copy(shard).start())
 
     add_part(z, lambda: None)
-
-    @pl.when(inner)
-    def _():
-        add_part(arrivals[0][0], lambda: None)
-
+    add_part(arrivals[0][0], lambda: None, inner)
     for k in range(1, n_sp - 1):
         settle(H, k)
         add_part(arrivals[k][0], functools.partial(settle, C, k))
 
-    for u in (Q, K, V, W, H, C):
-        own(u, lambda copy: copy.wait_send())
-        for k in range(n_sp - 1):
-            shard, target = arrivals[k]
-
-            @pl.when(forwards(k))
-            def _():
-                z_copy(u, shard, FWD, target).wait_send()
-
-            if u in (Q, K):
-                pair(u, shard, t).wait_send()
-    for i in range(len(others)):
-        n_copy(i).wait_send()
-        n_pair(i, t).wait_send()
-        for h in range(heads):
-            head_copy(h, i).wait_send()
-        for s in range(n_fs):
-            conv_copy(s, i).wait_send()
-    for i in range(per_core):
-        seq, (same, other) = q_copies(i)
-        other.wait_send()
-
-        @pl.when(seq != c)
-        def _():
-            same.wait_send()
+    for entry in sent[-RING:]:
+        drain(entry)
 
     @pl.when(z < n_sp - 1)
     def _():
@@ -746,35 +780,16 @@
     def _():
         down_copy.wait_send()
 
-    for index in range(heads + n_fs):
-        @pl.when(jnp.logical_not(inner))
-        def _():
-            up_copy_of(index, index).wait_send()
-
     @pl.when(inner)
     def _():
         back_copy.wait_send()
-
-    for shard in range(n_sp):
-        computed = inner | (shard != near)
-
-        @pl.when(computed)
-        def _():
-            for j in range(len(others)):
-                fin_copy(shard, j).wait_send()
-
-        @pl.when(computed & (shard // half_sp != t))
-        def _():
-            fin_copy(shard, len(others)).wait_send()
 
     for i in range(half_sp):
         shard = t * half_sp + i
         computed = inner | (shard != near)
 
         def arrived(core, j):
-            remote(
-                parts.at[0, pl.ds(0, rows), :], place(0, i), fin_send.at[0, j], fin_recv.at[core, i, j], {"tp": peer}
-            ).wait_recv()
+            arrive(remote(parts.at[0, pl.ds(0, rows), :], place(0, i), fin_recv.at[core, i, j], {"tp": peer}))
 
         @pl.when(computed)
         def _():
@@ -787,9 +802,7 @@
         @pl.when(jnp.logical_not(computed))
         def _():
             for core in range(n_tp):
-                remote(
-                    part_o, placed.at[0, :, lanes_at(i, n_fs * out_cols)], back_send.at[0], back_recv.at[core], {"tp": peer}
-                ).wait_recv()
+                arrive(remote(part_o, placed.at[0, :, lanes_at(i, n_fs * out_cols)], back_recv.at[core], {"tp": peer}))
     log_copy.wait()
 
 
@@ -842,12 +855,9 @@
         pltpu.VMEM((out_rows, n_fs * out_cols), BF16),
         pltpu.VMEM((rows, out_rows), BF16),
         pltpu.VMEM((rows, n_fs * out_cols), BF16),
-        dma((19,)), dma((6, n_sp)), dma((6, n_sp, 3)), dma((2, n_sp)), dma((2, n_sp)),
-        dma((3,)), dma((3,)), dma((3,)), dma((3,)), dma((n_fs,)), dma((n_fs // 2, 2)),
-        dma((heads, 3)), dma((heads, 3)), dma((2,)), dma((2,)), dma((n_fs, 3)), dma((n_fs, 3)),
-        dma((2, half_sp, 4)), dma((n_sp, 4)), dma((1 + half_sp,)),
-        dma((heads + n_fs,)), dma((heads + n_fs,)), dma((2,)), dma((1,)),
-        pltpu.SemaphoreType.REGULAR,
+        dma((10,)), dma((RING,)), dma((G + PIECES, n_sp - 1)), dma((2, n_sp - 1)), dma((2, 2)), dma((3,)), dma((n_fs,)),
+        dma((heads, 2)), dma((2,)), dma((2,)), dma((n_fs, 2)), dma((2, half_sp, 4)), dma((1 + half_sp,)),
+        dma((heads + n_fs,)), dma((2,)), dma((1,)), dma((2,)), dma((heads,)), dma((n_fs,)), dma((1,)),
     ]
     shapes = (
         jax.ShapeDtypeStruct((rows, half_sp * n_fs * out_cols), BF16),

time: 53.5 us -> 51.1 us (0.955)
  the two profiles are of different devices: /device:TPU:16 before, /device:TPU:1 now
where the time goes in v4:
time: 51.1 us; the launch traced here: 50.9 us
  Pallas kernels  50.3 us (98%)
  between operations  0.64 us (1%)
    pallas_call x1, Pallas kernels, fused_device(): pl.pallas_call(functools.partial(fused_kernel, n_sp), out_shape=(jax.Shap...  48.5 us
    pallas_call x1, Pallas kernels, fused_device(): pl.pallas_call(finish_kernel, out_shape=shapes, name='finish')(placed, logs)  1.81 us

profile of v4, /device:TPU:1, one launch (start us, length us, event | category | flops | bytes accessed | tf_op | source)
XLA Modules:
  0.0 50.9 jit_solution(13856347252560275808)
XLA Ops:
  0.6 48.5 %fused_layer.1 = (bf16[2,128,1024]{2,1,0:T(8,128)(2,1)}, f32[4,128]{1,0:T(4,128)}) custom-call(bf16[128,2048]{1,0:T(8,128)(2,1)} %tokens.1, bf16[2048]{0:T(1024)(128)(2,1)} %norm_gain_in.1, bf16[512,512]{1,0:T(8,128)(2,1)} %query_down.1, bf16[512]{0:T(512)(128)(2,1)} %query_gain_in.1, bf16[2048,256]{1,0:T(8,128)(2,1)} %latent_down.1, ...), custom_call_target="tpu_custom_call" | custom-call | tf_op jit(solution)/shard_map/fused_layer/pallas_call | solution.py:866
  49.1 1.8 %finish.1 = (bf16[128,1024]{1,0:T(8,128)(2,1)}, f32[4,128]{1,0:T(4,128)}) custom-call(bf16[2,128,1024]{2,1,0:T(8,128)(2,1)} %get-tuple-element.4.placed, f32[4,128]{1,0:T(4,128)} %get-tuple-element.5.log_in), custom_call_target="tpu_custom_call" | custom-call | tf_op jit(solution)/shard_map/finish/pallas_call | solution.py:877

commit v5 on v4

--- a/solution.py
+++ b/solution.py
@@ -222,9 +222,9 @@
     norm_gain, query_gain, latent_gain, conv_taps, group_gain, log_v,
     w_q, w_g, w_o, tok_v, lat_v, rope_v, qup_v, kup_v, vup_v, tab_v,
     normed, keys, key_tmp, q_out, q_lat, q_scr, g_acc, gated, low_rows, high_rows, padded,
-    mixed, parts, w_full, mixed_o, part_o,
+    mixed, parts, w_full, mixed_o, part_o, edge_in, head_acc,
     load_sem, ring_sem, z_recv, pair_recv, n_recv, np_recv, q_recv, head_recv, halo_recv, halo_send,
-    conv_recv, fin_recv, out_sem, up_recv, back_recv, back_send, nr_recv, hr_recv, cr_recv, corner_recv,
+    conv_recv, fin_recv, out_sem, up_recv, back_recv, back_send, nr_recv, hr_recv, cr_recv, corner_recv, edge_recv,
 ):
     z = lax.axis_index("sp")
     c = lax.axis_index("fs")
@@ -466,9 +466,9 @@
     for k in range(last):
         relay(K, k)
     share(Q, 0)
+    send_own(G + 2)
     relay(Q, last)
-    for p in range(2, PIECES):
-        send_own(G + p)
+    send_own(G + 3)
     for k in range(last):
         relay(G, k)
     share_normed(0)
@@ -486,6 +486,11 @@
 
     for i in range(len(others)):
         arrive(n_pair(i, peer))
+    halo = low_rows.shape[1]
+    edge_rows = pl.ds(pl.multiple_of(jnp.where(lower, rows - halo, 0), 16), halo)
+    edge_half = edge_in.at[:, :, lanes_at(t, half_width)]
+    edge_copy = remote(normed.at[:, edge_rows, lanes_at(t, half_width)], edge_half, edge_recv.at[0], {"sp": near})
+    edge_pair = remote(edge_half, edge_half, edge_recv.at[1], {"tp": peer})
     for k in range(n_sp - 1):
         arrive(pair(Q, arrivals[k][0], peer))
     seqs = normed[pl.ds(per_core * t, per_core)].reshape(per_core * rows, width)
@@ -503,15 +508,15 @@
 
     for name in ("hp", "cp"):
         loads[name].wait()
-    for u in (H, C):
-        send_own(u, at_end)
+    send_own(H, at_end)
+    send(edge_copy, at_end)
+    send_own(C, at_end)
 
     def add_shard(shard, first=False):
         rows_in = normed[:, :, lanes_at(shard, depth)].reshape(n_fs * rows, depth)
         term = dot(rows_in, w_g[shard])
         g_acc[...] = term if first else g_acc[...] + term
 
-    halo = low_rows.shape[1]
     up_copy = remote(
         gated.at[:, pl.ds(rows - halo, halo), :], low_rows, halo_recv.at[0], {"sp": z + 1}
     )(halo_send.at[0])
@@ -519,21 +524,34 @@
         gated.at[:, pl.ds(0, halo), :], high_rows, halo_recv.at[1], {"sp": z - 1}
     )(halo_send.at[1])
 
+    def add_arrival(k):
+        for p in range(PIECES):
+            settle(G + p, k)
+        add_shard(arrivals[k][0])
+
     def gate():
-        for k in range(n_sp - 1):
-            for p in range(PIECES):
-                settle(G + p, k)
-            add_shard(arrivals[k][0])
-        acc = g_acc[...]
-        gated[...] = (acc[:, 0:cols] * jax.nn.sigmoid(acc[:, cols : 2 * cols])).astype(BF16).reshape(n_fs, rows, cols)
-
-        @pl.when(z < n_sp - 1)
+        gated[...] = gate_of(g_acc[...]).reshape(n_fs, rows, cols)
+
+        @pl.when(inner)
         def _():
             up_copy.start()
-
-        @pl.when(z > 0)
+            down_copy.start()
+
+    def gate_of(acc):
+        return (acc[:, 0:cols] * jax.nn.sigmoid(acc[:, cols : 2 * cols])).astype(BF16)
+
+    def edge():
+        arrive(edge_pair)
+        acc = dot(edge_in[...].reshape(n_fs * halo, width), w_g[...].reshape(n_sp * depth, 2 * cols))
+        values = gate_of(acc).astype(F32).reshape(n_fs, halo, cols)
+
+        @pl.when(lower)
         def _():
-            down_copy.start()
+            padded[:, 0:halo, :] = values
+
+        @pl.when(jnp.logical_not(lower))
+        def _():
+            padded[:, halo + rows : 2 * halo + rows, :] = values
 
     for p in range(2):
         relay(G + p, last)
@@ -544,8 +562,12 @@
         relay(G + p, last)
     share(K, last)
 
+    add_arrival(0)
+
     @pl.when(inner)
     def _():
+        for k in range(1, n_sp - 1):
+            add_arrival(k)
         gate()
 
     for u in (H, C):
@@ -594,10 +616,10 @@
         ref = mixed.at[others[i], :, pl.ds(h * VDIM, VDIM)]
         return i, remote(ref, ref, hr_recv.at[h], {"fs": others[1 - i]})
 
-    def pass_head(h):
+    def pass_head(h, cond):
         i, copy = head_relay(h)
-        arrive(head_copy(h, i))
-        send(copy)
+        when(cond, lambda: arrive(head_copy(h, i)))
+        send(copy, cond)
 
     whole = q_scr[...]
     shifted = pltpu.roll(whole, whole.shape[1] - ROPE, 1)
@@ -613,24 +635,35 @@
         for i in range(2):
             send(head_copy(h, i))
         send(to_near(h), at_end)
-        if h == 0:
-            pass_on(C, outer, far)
+        if h == 1:
+            when(inner, lambda: arrive(edge_copy))
+            send(edge_pair, inner)
     log_v[...] = jnp.transpose(logs)[0:heads, :]
     log_copy = pltpu.make_async_copy(log_v, log_out, out_sem.at[0])
     log_copy.start()
     pass_on(H, far, outer)
+
+    @pl.when(at_end)
+    def _():
+        for k in range(1, last):
+            add_arrival(k)
+
     for h in range(heads):
-        pass_head(h)
-    pass_on(C, far, outer)
+        pass_head(h, at_end)
 
     @pl.when(at_end)
     def _():
+        add_arrival(last)
         gate()
+
+    @pl.when(inner)
+    def _():
+        edge()
 
     reach = conv_taps.shape[0] // 2
     padded[:, halo : halo + rows, :] = gated[...].astype(F32)
 
-    @pl.when(z > 0)
+    @pl.when(z > 1)
     def _():
         up_copy.wait_recv()
         padded[:, 0:halo, :] = low_rows[...].astype(F32)
@@ -639,7 +672,7 @@
     def _():
         padded[:, 0:halo, :] = jnp.zeros((n_fs, halo, cols), F32)
 
-    @pl.when(z < n_sp - 1)
+    @pl.when(z < n_sp - 2)
     def _():
         down_copy.wait_recv()
         padded[:, halo + rows : 2 * halo + rows, :] = high_rows[...].astype(F32)
@@ -672,8 +705,6 @@
     gains = all_gains[:, 0:cols]
     for i in range(1, n_fs):
         gains = jnp.where(c == i, all_gains[:, i * cols : (i + 1) * cols], gains)
-    relay(H, last)
-
     def conv_seq(s):
         filtered = jnp.zeros((rows, cols), F32)
         for j in range(conv_taps.shape[0]):
@@ -695,6 +726,11 @@
     send(to_near(heads + c), at_end)
     for s, i in ((c, 0), (c_d, 1), (c_y, 0), (c, 1), (c_d, 0), (c_x, 1)):
         send(conv_copy(s, i))
+    pass_on(C, outer, far)
+    pass_on(C, far, outer)
+    for h in range(heads):
+        pass_head(h, inner)
+    relay(H, last)
     arrive(conv_copy(c, 0))
     send(to_near(heads + c_x), at_end)
     arrive(conv_copy(c, 1))
@@ -702,10 +738,74 @@
     send(conv_relay(c, 1))
     arrive(conv_corner_in())
     send(to_near(heads + c_d), at_end)
-    relay(C, last)
     for s, i in ((c_x, 0), (c_d, 1)):
         arrive(conv_copy(s, i))
         send(conv_relay(s, i))
+    relay(C, last)
+    for h in range(heads):
+        arrive(head_copy(h, 1 - head_relay(h)[0]))
+        arrive(head_relay(h)[1])
+
+    def head_part(shard):
+        head_acc[shard] = dot(mixed[:, :, 0:head_rows].reshape(n_fs * rows, head_rows), w_o[shard, 0:head_rows, :])
+
+    head_part(z)
+    settle(H, 1)
+    head_part(arrivals[1][0])
+
+    @pl.when(inner)
+    def _():
+        head_part(arrivals[0][0])
+        for k in range(2, n_sp - 1):
+            head_part(arrivals[k][0])
+
+    for s, i in ((c_y, 1), (c_d, 0), (c_x, 1), (c_y, 0)):
+        arrive(conv_copy(s, i))
+    for s in others:
+        arrive(conv_relay(s, 0))
+
+    def place(core, shard):
+        first = (shard % half_sp) * (n_fs * out_cols) + c * out_cols
+        return placed.at[core, :, pl.ds(pl.multiple_of(first, LANES), out_cols)]
+
+    def fin_copy(shard, j):
+        seq = others[j] if j < len(others) else c
+        return remote(
+            parts.at[shard, pl.ds(pl.multiple_of(seq * rows, LANES), rows), :], place(t, shard),
+            fin_recv.at[t, shard % half_sp, j], {"fs": seq, "tp": shard // half_sp},
+        )
+
+    def keep_copy(shard):
+        ref = parts.at[shard, pl.ds(pl.multiple_of(c * rows, LANES), rows), :]
+        return pltpu.make_async_copy(ref, place(t, shard), out_sem.at[1 + shard % half_sp])
+
+    def add_part(shard, cond=None):
+        def compute():
+            part = head_acc[shard] + dot(
+                mixed[:, :, head_rows:out_rows].reshape(n_fs * rows, out_rows - head_rows), w_o[shard, head_rows:out_rows, :]
+            )
+            parts[shard] = part.astype(BF16)
+
+        when(cond, compute)
+        for j in (2, 0, 1):
+            send(fin_copy(shard, j), cond)
+        mine = shard // half_sp == t
+        send(fin_copy(shard, len(others)), both(cond, jnp.logical_not(mine)))
+        when(both(cond, mine), lambda: keep_copy(shard).start())
+
+    add_part(z)
+    add_part(arrivals[0][0], inner)
+    settle(C, 1)
+    add_part(arrivals[1][0])
+    for k in range(2, n_sp - 1):
+        settle(H, k)
+
+        @pl.when(at_end)
+        def _():
+            head_part(arrivals[k][0])
+
+        settle(C, k)
+        add_part(arrivals[k][0])
 
     back_lanes = lanes_at(z % half_sp, n_fs * out_cols)
     back_copy = remote(
@@ -724,64 +824,13 @@
     def _():
         neighbour_part()
 
-    for h in range(heads):
-        arrive(head_copy(h, 1 - head_relay(h)[0]))
-        arrive(head_relay(h)[1])
-    for s, i in ((c_y, 1), (c_d, 0), (c_x, 1), (c_y, 0)):
-        arrive(conv_copy(s, i))
-    for s in others:
-        arrive(conv_relay(s, 0))
-
-    def place(core, shard):
-        first = (shard % half_sp) * (n_fs * out_cols) + c * out_cols
-        return placed.at[core, :, pl.ds(pl.multiple_of(first, LANES), out_cols)]
-
-    def fin_copy(shard, j):
-        seq = others[j] if j < len(others) else c
-        return remote(
-            parts.at[shard, pl.ds(pl.multiple_of(seq * rows, LANES), rows), :], place(t, shard),
-            fin_recv.at[t, shard % half_sp, j], {"fs": seq, "tp": shard // half_sp},
-        )
-
-    def keep_copy(shard):
-        ref = parts.at[shard, pl.ds(pl.multiple_of(c * rows, LANES), rows), :]
-        return pltpu.make_async_copy(ref, place(t, shard), out_sem.at[1 + shard % half_sp])
-
-    def add_part(shard, between, cond=None):
-        def compute():
-            part = dot(mixed[:, :, 0:head_rows].reshape(n_fs * rows, head_rows), w_o[shard, 0:head_rows, :])
-            between()
-            part = part + dot(
-                mixed[:, :, head_rows:out_rows].reshape(n_fs * rows, out_rows - head_rows), w_o[shard, head_rows:out_rows, :]
-            )
-            parts[shard] = part.astype(BF16)
-
-        when(cond, compute)
-        for j in (2, 0, 1):
-            send(fin_copy(shard, j), cond)
-        mine = shard // half_sp == t
-        send(fin_copy(shard, len(others)), both(cond, jnp.logical_not(mine)))
-        when(both(cond, mine), lambda: keep_copy(shard).start())
-
-    add_part(z, lambda: None)
-    add_part(arrivals[0][0], lambda: None, inner)
-    for k in range(1, n_sp - 1):
-        settle(H, k)
-        add_part(arrivals[k][0], functools.partial(settle, C, k))
-
     for entry in sent[-RING:]:
         drain(entry)
 
-    @pl.when(z < n_sp - 1)
+    @pl.when(inner)
     def _():
         up_copy.wait_send()
-
-    @pl.when(z > 0)
-    def _():
         down_copy.wait_send()
-
-    @pl.when(inner)
-    def _():
         back_copy.wait_send()
 
     for i in range(half_sp):
@@ -855,9 +904,11 @@
         pltpu.VMEM((out_rows, n_fs * out_cols), BF16),
         pltpu.VMEM((rows, out_rows), BF16),
         pltpu.VMEM((rows, n_fs * out_cols), BF16),
+        pltpu.VMEM((n_fs, halo, width), BF16),
+        pltpu.VMEM((n_sp, n_fs * rows, out_cols), F32),
         dma((10,)), dma((RING,)), dma((G + PIECES, n_sp - 1)), dma((2, n_sp - 1)), dma((2, 2)), dma((3,)), dma((n_fs,)),
         dma((heads, 2)), dma((2,)), dma((2,)), dma((n_fs, 2)), dma((2, half_sp, 4)), dma((1 + half_sp,)),
-        dma((heads + n_fs,)), dma((2,)), dma((1,)), dma((2,)), dma((heads,)), dma((n_fs,)), dma((1,)),
+        dma((heads + n_fs,)), dma((2,)), dma((1,)), dma((2,)), dma((heads,)), dma((n_fs,)), dma((1,)), dma((2,)),
     ]
     shapes = (
         jax.ShapeDtypeStruct((rows, half_sp * n_fs * out_cols), BF16),

time: 51.1 us -> 50.3 us (0.984)
  Pallas kernels: 50.3 us -> 49.5 us
    pallas_call x1, Pallas kernels: 48.5 us -> 47.7 us  [fused_device(): pl.pallas_call(functools.partial(fused_kernel, n_sp), out_shape=(jax.Shap...]
where the time goes in v5:
time: 50.3 us; the launch traced here: 50.2 us
  Pallas kernels  49.5 us (98%)
  between operations  0.64 us (1%)
    pallas_call x1, Pallas kernels, fused_device(): pl.pallas_call(functools.partial(fused_kernel, n_sp), out_shape=(jax.Shap...  47.7 us
    pallas_call x1, Pallas kernels, fused_device(): pl.pallas_call(finish_kernel, out_shape=shapes, name='finish')(placed, logs)  1.81 us

profile of v5, /device:TPU:1, one launch (start us, length us, event | category | flops | bytes accessed | tf_op | source)
XLA Modules:
  0.0 50.2 jit_solution(15531567418475120556)
XLA Ops:
  0.6 47.7 %fused_layer.1 = (bf16[2,128,1024]{2,1,0:T(8,128)(2,1)}, f32[4,128]{1,0:T(4,128)}) custom-call(bf16[128,2048]{1,0:T(8,128)(2,1)} %tokens.1, bf16[2048]{0:T(1024)(128)(2,1)} %norm_gain_in.1, bf16[512,512]{1,0:T(8,128)(2,1)} %query_down.1, bf16[512]{0:T(512)(128)(2,1)} %query_gain_in.1, bf16[2048,256]{1,0:T(8,128)(2,1)} %latent_down.1, ...), custom_call_target="tpu_custom_call" | custom-call | tf_op jit(solution)/shard_map/fused_layer/pallas_call | solution.py:917
  48.4 1.8 %finish.1 = (bf16[128,1024]{1,0:T(8,128)(2,1)}, f32[4,128]{1,0:T(4,128)}) custom-call(bf16[2,128,1024]{2,1,0:T(8,128)(2,1)} %get-tuple-element.4.placed, f32[4,128]{1,0:T(4,128)} %get-tuple-element.5.log_in), custom_call_target="tpu_custom_call" | custom-call | tf_op jit(solution)/shard_map/finish/pallas_call | solution.py:928

commit v6 on v5

--- a/solution.py
+++ b/solution.py
@@ -182,7 +182,7 @@
 BF16 = jnp.bfloat16
 Q, K, H, C, G = range(5)
 PIECES = 4
-RING = 32
+RING = 24
 
 
 def rope_tables(length):
@@ -221,7 +221,7 @@
     placed, log_out,
     norm_gain, query_gain, latent_gain, conv_taps, group_gain, log_v,
     w_q, w_g, w_o, tok_v, lat_v, rope_v, qup_v, kup_v, vup_v, tab_v,
-    normed, keys, key_tmp, q_out, q_lat, q_scr, g_acc, gated, low_rows, high_rows, padded,
+    normed, keys, rope_keys, key_tmp, q_out, q_lat, q_scr, g_acc, gated, low_rows, high_rows, padded,
     mixed, parts, w_full, mixed_o, part_o, edge_in, head_acc,
     load_sem, ring_sem, z_recv, pair_recv, n_recv, np_recv, q_recv, head_recv, halo_recv, halo_send,
     conv_recv, fin_recv, out_sem, up_recv, back_recv, back_send, nr_recv, hr_recv, cr_recv, corner_recv, edge_recv,
@@ -354,7 +354,7 @@
         if u == Q:
             return w_q.at[shard, half(side, q_half), :]
         if u == K:
-            return keys.at[shard, half(side, k_half), :]
+            return keys.at[shard, side]
         if u == H:
             return w_o.at[shard, pl.ds(0, head_rows), :]
         if u == C:
@@ -392,6 +392,10 @@
     def relay(u, k):
         pass_on(u, *arrivals[k])
 
+    def both_ways(u):
+        pass_on(u, outer, far)
+        pass_on(u, far, outer)
+
     def settle(u, k):
         when(at_end, lambda: z_arrive(u, arrivals[k][0]))
 
@@ -447,42 +451,46 @@
     loads["lg"].wait()
     own_normed = normed[c]
     latent = rms_scale(dot(own_normed, lat_v[...]), row_of(latent_gain))
-    keys[z, :, 0:KVR] = latent.astype(BF16)
+    keys[z, :, 0:k_half, :] = latent.astype(BF16).reshape(n_tp, k_half, KVR)
     loads["rope"].wait()
     loads["tab"].wait()
     key_tmp[...] = jnp.zeros_like(key_tmp)
     key_tmp[:, 0:ROPE] = dot_nt(own_normed, rope_v[...])
-    keys[z, :, KVR : KVR + LANES] = rotate_lanes(key_tmp[...]).astype(BF16)
+    rotated = rotate_lanes(key_tmp[...])
+    fold = KVR // ROPE
+    strip = k_half // fold
+    for side in range(n_tp):
+        for pair_of in range(fold // 2):
+            first = side * k_half + 2 * pair_of * strip
+            packed = rotated[first : first + strip, :] + pltpu.roll(
+                rotated[first + strip : first + 2 * strip, :], ROPE, 1
+            )
+            keys[z, side, k_half : k_half + strip, pair_of * LANES : (pair_of + 1) * LANES] = packed.astype(BF16)
     send_own(K)
     send_own(G)
+    send_own(G + 1)
     load_rest()
 
     last = n_sp - 2
-    for k in range(last):
-        relay(Q, k)
-    send_own(G + 1)
+    both_ways(Q)
     pass_normed(0)
     pass_normed(1)
-    for k in range(last):
-        relay(K, k)
+    both_ways(K)
     share(Q, 0)
     send_own(G + 2)
     relay(Q, last)
     send_own(G + 3)
-    for k in range(last):
-        relay(G, k)
+    both_ways(G)
     share_normed(0)
     share_normed(1)
     relay(K, last)
-    for k in range(last):
-        relay(G + 1, k)
+    both_ways(G + 1)
     for k in range(1, last):
         share(Q, k)
     share_normed(2)
     share(Q, last)
     for p in range(2, PIECES):
-        for k in range(last):
-            relay(G + p, k)
+        both_ways(G + p)
 
     for i in range(len(others)):
         arrive(n_pair(i, peer))
@@ -564,14 +572,15 @@
 
     add_arrival(0)
 
+    send_own(H, inner)
+
     @pl.when(inner)
     def _():
         for k in range(1, n_sp - 1):
             add_arrival(k)
         gate()
 
-    for u in (H, C):
-        send_own(u, inner)
+    send_own(C, inner)
     for name in ("qup", "kup", "vup", "qg", "taps", "gg"):
         loads[name].wait()
 
@@ -586,6 +595,17 @@
     q_scr[...] = dot(latent_query, qup_v[...])
     for k in range(n_sp - 1):
         arrive(pair(K, arrivals[k][0], peer))
+
+    key_lane = lax.broadcasted_iota(jnp.int32, (strip, LANES), 1)
+    for shard in range(n_sp):
+        for side in range(n_tp):
+            for pair_of in range(fold // 2):
+                packed = keys[
+                    shard, side, k_half : k_half + strip, pair_of * LANES : (pair_of + 1) * LANES
+                ].astype(F32)
+                for part, values in enumerate((packed, pltpu.roll(packed, ROPE, 1))):
+                    first = (shard * n_tp + side) * k_half + (2 * pair_of + part) * strip
+                    rope_keys[first : first + strip, :] = jnp.where(key_lane < ROPE, values, 0.0).astype(BF16)
 
     def attend(h, shifted):
         start = h * (NOPE + ROPE)
@@ -595,31 +615,31 @@
         plain = source[:, start : start + NOPE].astype(BF16)
         rope_part = rotate_lanes(source[:, start + NOPE : start + NOPE + LANES]).astype(BF16)
         absorbed = dot_nt(plain, kup_v[:, h * NOPE : (h + 1) * NOPE]).astype(BF16)
-        query = jnp.concatenate([absorbed, rope_part], axis=1)
-        all_keys = keys[...].reshape(n_sp * rows, KVR + LANES)
-        scores = dot_nt(query, all_keys) * (NOPE + ROPE) ** (-0.5)
+        latents = keys[:, :, 0:k_half, :].reshape(n_sp * rows, KVR)
+        scores = (dot_nt(absorbed, latents) + dot_nt(rope_part, rope_keys[...])) * (NOPE + ROPE) ** (-0.5)
         row_max = jnp.max(scores, axis=1, keepdims=True)
         weights = jnp.exp(scores - row_max)
         total = jnp.sum(weights, axis=1, keepdims=True)
-        added = dot(weights.astype(BF16), all_keys[:, 0:KVR])
+        added = dot(weights.astype(BF16), latents)
         attended = (added / total).astype(BF16)
         head_out = dot(attended, vup_v[:, h * VDIM : (h + 1) * VDIM])
         mixed[c, :, h * VDIM : (h + 1) * VDIM] = head_out.astype(BF16)
         return row_max + jnp.log(total)
 
+    def head_ref(owner, h):
+        return mixed.at[owner, :, pl.ds(2 * h * VDIM, 2 * VDIM)]
+
     def head_copy(h, i):
-        ref = mixed.at[c, :, pl.ds(h * VDIM, VDIM)]
+        ref = head_ref(c, h)
         return remote(ref, ref, head_recv.at[h, i], {"fs": others[i]})
 
     def head_relay(h):
-        i = h * 2 // heads
-        ref = mixed.at[others[i], :, pl.ds(h * VDIM, VDIM)]
-        return i, remote(ref, ref, hr_recv.at[h], {"fs": others[1 - i]})
+        ref = head_ref(others[h], h)
+        return remote(ref, ref, hr_recv.at[h], {"fs": others[1 - h]})
 
     def pass_head(h, cond):
-        i, copy = head_relay(h)
-        when(cond, lambda: arrive(head_copy(h, i)))
-        send(copy, cond)
+        when(cond, lambda: arrive(head_copy(h, h)))
+        send(head_relay(h), cond)
 
     whole = q_scr[...]
     shifted = pltpu.roll(whole, whole.shape[1] - ROPE, 1)
@@ -627,14 +647,16 @@
     logs = jnp.zeros((rows, LANES), F32)
 
     def to_near(group):
-        ref = mixed.at[c, :, lanes_at(group, cols)]
-        return remote(ref, mixed_o.at[:, lanes_at(group, cols)], up_recv.at[group], {"sp": near})
+        lanes = lanes_at(group, cols) if isinstance(group, jax.Array) or group >= heads else pl.ds(2 * group * cols, 2 * cols)
+        index = group - heads + 2 if isinstance(group, jax.Array) or group >= heads else group
+        return remote(mixed.at[c, :, lanes], mixed_o.at[:, lanes], up_recv.at[index], {"sp": near})
 
     for h in range(heads):
         logs = jnp.where(lane == h, attend(h, shifted), logs)
-        for i in range(2):
-            send(head_copy(h, i))
-        send(to_near(h), at_end)
+        if h % 2:
+            for i in range(2):
+                send(head_copy(h // 2, i))
+            send(to_near(h // 2), at_end)
         if h == 1:
             when(inner, lambda: arrive(edge_copy))
             send(edge_pair, inner)
@@ -648,7 +670,7 @@
         for k in range(1, last):
             add_arrival(k)
 
-    for h in range(heads):
+    for h in range(2):
         pass_head(h, at_end)
 
     @pl.when(at_end)
@@ -728,7 +750,7 @@
         send(conv_copy(s, i))
     pass_on(C, outer, far)
     pass_on(C, far, outer)
-    for h in range(heads):
+    for h in range(2):
         pass_head(h, inner)
     relay(H, last)
     arrive(conv_copy(c, 0))
@@ -742,9 +764,9 @@
         arrive(conv_copy(s, i))
         send(conv_relay(s, i))
     relay(C, last)
-    for h in range(heads):
-        arrive(head_copy(h, 1 - head_relay(h)[0]))
-        arrive(head_relay(h)[1])
+    for h in range(2):
+        arrive(head_copy(h, 1 - h))
+        arrive(head_relay(h))
 
     def head_part(shard):
         head_acc[shard] = dot(mixed[:, :, 0:head_rows].reshape(n_fs * rows, head_rows), w_o[shard, 0:head_rows, :])
@@ -793,6 +815,23 @@
         send(fin_copy(shard, len(others)), both(cond, jnp.logical_not(mine)))
         when(both(cond, mine), lambda: keep_copy(shard).start())
 
+    back_lanes = lanes_at(z % half_sp, n_fs * out_cols)
+    back_copy = remote(
+        part_o, placed.at[t, :, back_lanes], back_recv.at[t], {"sp": outer, "tp": z // half_sp}
+    )(back_send.at[0])
+    for name in ("hf", "cf"):
+        loads[name].wait()
+
+    def neighbour_part():
+        for i in (0, 1, *range(heads, heads + n_fs)):
+            arrive(to_near(i))
+        part_o[...] = dot(mixed_o[...], w_full[...]).astype(BF16)
+        back_copy.start()
+
+    @pl.when(inner)
+    def _():
+        neighbour_part()
+
     add_part(z)
     add_part(arrivals[0][0], inner)
     settle(C, 1)
@@ -806,23 +845,6 @@
 
         settle(C, k)
         add_part(arrivals[k][0])
-
-    back_lanes = lanes_at(z % half_sp, n_fs * out_cols)
-    back_copy = remote(
-        part_o, placed.at[t, :, back_lanes], back_recv.at[t], {"sp": outer, "tp": z // half_sp}
-    )(back_send.at[0])
-    for name in ("hf", "cf"):
-        loads[name].wait()
-
-    def neighbour_part():
-        for i in range(heads + n_fs):
-            arrive(to_near(i))
-        part_o[...] = dot(mixed_o[...], w_full[...]).astype(BF16)
-        back_copy.start()
-
-    @pl.when(inner)
-    def _():
-        neighbour_part()
 
     for entry in sent[-RING:]:
         drain(entry)
@@ -889,7 +911,8 @@
         like(tokens), like(latent_down), pltpu.VMEM(rope_down.shape[::-1], BF16), like(query_up), like(key_up), like(value_up),
         pltpu.VMEM((3, rows, LANES), F32),
         pltpu.VMEM((n_fs, rows, width), BF16),
-        pltpu.VMEM((n_sp, rows, KVR + LANES), BF16),
+        pltpu.VMEM((n_sp, 2, rows // 2 + rows // 2 * ROPE // KVR, KVR), BF16),
+        pltpu.VMEM((n_sp * rows, LANES), BF16),
         pltpu.VMEM((rows, LANES), F32),
         pltpu.VMEM((n_fs // 2, rows, q_cols), F32),
         pltpu.VMEM((n_fs, rows, q_cols), F32),
@@ -907,8 +930,8 @@
         pltpu.VMEM((n_fs, halo, width), BF16),
         pltpu.VMEM((n_sp, n_fs * rows, out_cols), F32),
         dma((10,)), dma((RING,)), dma((G + PIECES, n_sp - 1)), dma((2, n_sp - 1)), dma((2, 2)), dma((3,)), dma((n_fs,)),
-        dma((heads, 2)), dma((2,)), dma((2,)), dma((n_fs, 2)), dma((2, half_sp, 4)), dma((1 + half_sp,)),
-        dma((heads + n_fs,)), dma((2,)), dma((1,)), dma((2,)), dma((heads,)), dma((n_fs,)), dma((1,)), dma((2,)),
+        dma((2, 2)), dma((2,)), dma((2,)), dma((n_fs, 2)), dma((2, half_sp, 4)), dma((1 + half_sp,)),
+        dma((2 + n_fs,)), dma((2,)), dma((1,)), dma((2,)), dma((2,)), dma((n_fs,)), dma((1,)), dma((2,)),
     ]
     shapes = (
         jax.ShapeDtypeStruct((rows, half_sp * n_fs * out_cols), BF16),

time: 50.3 us -> 48.7 us (0.968)
  Pallas kernels: 49.5 us -> 47.9 us
    pallas_call x1, Pallas kernels: 47.7 us -> 46.1 us  [fused_device(): pl.pallas_call(functools.partial(fused_kernel, n_sp), out_shape=(jax.Shap...]
where the time goes in v6:
time: 48.7 us; the launch traced here: 48.6 us
  Pallas kernels  47.9 us (98%)
  between operations  0.64 us (1%)
    pallas_call x1, Pallas kernels, fused_device(): pl.pallas_call(functools.partial(fused_kernel, n_sp), out_shape=(jax.Shap...  46.1 us
    pallas_call x1, Pallas kernels, fused_device(): pl.pallas_call(finish_kernel, out_shape=shapes, name='finish')(placed, logs)  1.81 us

profile of v6, /device:TPU:1, one launch (start us, length us, event | category | flops | bytes accessed | tf_op | source)
XLA Modules:
  0.0 48.6 jit_solution(12053487225945544735)
XLA Ops:
  0.6 46.1 %fused_layer.1 = (bf16[2,128,1024]{2,1,0:T(8,128)(2,1)}, f32[4,128]{1,0:T(4,128)}) custom-call(bf16[128,2048]{1,0:T(8,128)(2,1)} %tokens.1, bf16[2048]{0:T(1024)(128)(2,1)} %norm_gain_in.1, bf16[512,512]{1,0:T(8,128)(2,1)} %query_down.1, bf16[512]{0:T(512)(128)(2,1)} %query_gain_in.1, bf16[2048,256]{1,0:T(8,128)(2,1)} %latent_down.1, ...), custom_call_target="tpu_custom_call" | custom-call | tf_op jit(solution)/shard_map/fused_layer/pallas_call | solution.py:940
  46.8 1.8 %finish.1 = (bf16[128,1024]{1,0:T(8,128)(2,1)}, f32[4,128]{1,0:T(4,128)}) custom-call(bf16[2,128,1024]{2,1,0:T(8,128)(2,1)} %get-tuple-element.4.placed, f32[4,128]{1,0:T(4,128)} %get-tuple-element.5.log_in), custom_call_target="tpu_custom_call" | custom-call | tf_op jit(solution)/shard_map/finish/pallas_call | solution.py:951

commit v7 on v6

--- a/solution.py
+++ b/solution.py
@@ -182,7 +182,7 @@
 BF16 = jnp.bfloat16
 Q, K, H, C, G = range(5)
 PIECES = 4
-RING = 24
+RING = 20
 
 
 def rope_tables(length):
@@ -224,7 +224,7 @@
     normed, keys, rope_keys, key_tmp, q_out, q_lat, q_scr, g_acc, gated, low_rows, high_rows, padded,
     mixed, parts, w_full, mixed_o, part_o, edge_in, head_acc,
     load_sem, ring_sem, z_recv, pair_recv, n_recv, np_recv, q_recv, head_recv, halo_recv, halo_send,
-    conv_recv, fin_recv, out_sem, up_recv, back_recv, back_send, nr_recv, hr_recv, cr_recv, corner_recv, edge_recv,
+    conv_recv, fin_recv, out_sem, up_recv, back_recv, back_send, nr_recv, corner_recv, edge_recv,
 ):
     z = lax.axis_index("sp")
     c = lax.axis_index("fs")
@@ -336,6 +336,9 @@
     def arrive(make):
         make(ring_sem.at[0]).wait_recv()
 
+    def arrive_all(like, recv_sem):
+        arrive(remote(like, like, recv_sem, {"tp": peer}))
+
     q_half = depth // n_tp
     piece = depth // PIECES
     k_half = rows // n_tp
@@ -401,7 +404,7 @@
 
     def pair(u, shard, side):
         ref = block(u, shard, side)
-        return remote(ref, ref, pair_recv.at[u, slot_of(shard, z)], {"tp": peer})
+        return remote(ref, ref, pair_recv.at[u], {"tp": peer})
 
     def share(u, k):
         settle(u, k)
@@ -422,7 +425,7 @@
 
     def n_pair(i, side):
         ref = normed.at[others[i], :, lanes_at(side, half_width)]
-        return remote(ref, ref, np_recv.at[i], {"tp": peer})
+        return remote(ref, ref, np_recv.at[0], {"tp": peer})
 
     def pass_normed(i):
         arrive(n_copy(i, i))
@@ -492,22 +495,20 @@
     for p in range(2, PIECES):
         both_ways(G + p)
 
-    for i in range(len(others)):
-        arrive(n_pair(i, peer))
+    arrive_all(normed.at[pl.ds(0, n_fs - 1), :, lanes_at(peer, half_width)], np_recv.at[0])
     halo = low_rows.shape[1]
     edge_rows = pl.ds(pl.multiple_of(jnp.where(lower, rows - halo, 0), 16), halo)
     edge_half = edge_in.at[:, :, lanes_at(t, half_width)]
     edge_copy = remote(normed.at[:, edge_rows, lanes_at(t, half_width)], edge_half, edge_recv.at[0], {"sp": near})
     edge_pair = remote(edge_half, edge_half, edge_recv.at[1], {"tp": peer})
-    for k in range(n_sp - 1):
-        arrive(pair(Q, arrivals[k][0], peer))
+    arrive_all(w_q.at[pl.ds(0, n_sp - 1), half(peer, q_half), :], pair_recv.at[Q])
     seqs = normed[pl.ds(per_core * t, per_core)].reshape(per_core * rows, width)
     q_out[...] = dot(seqs, w_q[...].reshape(n_sp * depth, q_cols)).reshape(per_core, rows, q_cols)
 
     for i in range(per_core):
         seq = per_core * t + i
         for core in (peer, t):
-            copy = remote(q_out.at[i], q_lat.at[c], q_recv.at[c], {"fs": seq, "tp": core})
+            copy = remote(q_out.at[i], q_lat.at[c], q_recv.at[0], {"fs": seq, "tp": core})
             send(copy, None if core is peer else seq != c)
 
         @pl.when(seq == c)
@@ -584,17 +585,21 @@
     for name in ("qup", "kup", "vup", "qg", "taps", "gg"):
         loads[name].wait()
 
-    for source in range(n_fs):
-        @pl.when((c != source) | (t != c // per_core))
-        def _():
-            arrive(remote(q_out.at[0], q_lat.at[source], q_recv.at[source], {"tp": peer}))
+    here = t == c // per_core
+
+    @pl.when(here)
+    def _():
+        arrive_all(q_lat.at[pl.ds(0, n_fs - 1)], q_recv.at[0])
+
+    @pl.when(jnp.logical_not(here))
+    def _():
+        arrive_all(q_lat, q_recv.at[0])
 
     pass_on(H, outer, far)
     whole_q = jnp.concatenate([q_lat[i] for i in range(n_fs)], axis=1)
     latent_query = rms_scale(whole_q, row_of(query_gain)).astype(BF16)
     q_scr[...] = dot(latent_query, qup_v[...])
-    for k in range(n_sp - 1):
-        arrive(pair(K, arrivals[k][0], peer))
+    arrive_all(keys.at[pl.ds(0, n_sp - 1), peer], pair_recv.at[K])
 
     key_lane = lax.broadcasted_iota(jnp.int32, (strip, LANES), 1)
     for shard in range(n_sp):
@@ -631,11 +636,11 @@
 
     def head_copy(h, i):
         ref = head_ref(c, h)
-        return remote(ref, ref, head_recv.at[h, i], {"fs": others[i]})
+        return remote(ref, ref, head_recv.at[h if h == i else 2], {"fs": others[i]})
 
     def head_relay(h):
         ref = head_ref(others[h], h)
-        return remote(ref, ref, hr_recv.at[h], {"fs": others[1 - h]})
+        return remote(ref, ref, head_recv.at[2], {"fs": others[1 - h]})
 
     def pass_head(h, cond):
         when(cond, lambda: arrive(head_copy(h, h)))
@@ -648,8 +653,7 @@
 
     def to_near(group):
         lanes = lanes_at(group, cols) if isinstance(group, jax.Array) or group >= heads else pl.ds(2 * group * cols, 2 * cols)
-        index = group - heads + 2 if isinstance(group, jax.Array) or group >= heads else group
-        return remote(mixed.at[c, :, lanes], mixed_o.at[:, lanes], up_recv.at[index], {"sp": near})
+        return remote(mixed.at[c, :, lanes], mixed_o.at[:, lanes], up_recv.at[0], {"sp": near})
 
     for h in range(heads):
         logs = jnp.where(lane == h, attend(h, shifted), logs)
@@ -706,9 +710,9 @@
     def conv_ref(s, group):
         return mixed.at[s, :, pl.ds(pl.multiple_of(head_rows + group * cols, LANES), cols)]
 
-    def conv_copy(s, i):
+    def conv_copy(s, i, slot=4):
         ref = conv_ref(s, c)
-        return remote(ref, ref, conv_recv.at[s, i], {"fs": others[i]})
+        return remote(ref, ref, conv_recv.at[slot], {"fs": others[i]})
 
     def conv_corner():
         ref = conv_ref(c_d, c)
@@ -720,7 +724,7 @@
 
     def conv_relay(s, i):
         ref = conv_ref(s, others[i])
-        return remote(ref, ref, cr_recv.at[s], {"fs": others[1 - i]})
+        return remote(ref, ref, conv_recv.at[4], {"fs": others[1 - i]})
 
     taps = conv_taps[...].astype(F32)
     all_gains = row_of(group_gain).astype(F32)
@@ -741,32 +745,30 @@
     conv_seq(c_d)
     send(conv_corner())
     conv_seq(c_x)
-    send(conv_copy(c_x, 0))
+    send(conv_copy(c_x, 0, 0))
     conv_seq(c_y)
-    send(conv_copy(c_y, 1))
+    send(conv_copy(c_y, 1, 2))
     conv_seq(c)
     send(to_near(heads + c), at_end)
-    for s, i in ((c, 0), (c_d, 1), (c_y, 0), (c, 1), (c_d, 0), (c_x, 1)):
-        send(conv_copy(s, i))
+    for s, i, slot in ((c, 0, 1), (c_d, 1, 4), (c_y, 0, 4), (c, 1, 4), (c_d, 0, 4), (c_x, 1, 3)):
+        send(conv_copy(s, i, slot))
     pass_on(C, outer, far)
     pass_on(C, far, outer)
     for h in range(2):
         pass_head(h, inner)
     relay(H, last)
-    arrive(conv_copy(c, 0))
+    arrive(conv_copy(c, 0, 0))
     send(to_near(heads + c_x), at_end)
-    arrive(conv_copy(c, 1))
+    arrive(conv_copy(c, 1, 2))
     send(to_near(heads + c_y), at_end)
     send(conv_relay(c, 1))
     arrive(conv_corner_in())
     send(to_near(heads + c_d), at_end)
-    for s, i in ((c_x, 0), (c_d, 1)):
-        arrive(conv_copy(s, i))
+    for s, i, slot in ((c_x, 0, 1), (c_d, 1, 3)):
+        arrive(conv_copy(s, i, slot))
         send(conv_relay(s, i))
     relay(C, last)
-    for h in range(2):
-        arrive(head_copy(h, 1 - h))
-        arrive(head_relay(h))
+    arrive_all(parts.at[pl.ds(0, 2)], head_recv.at[2])
 
     def head_part(shard):
         head_acc[shard] = dot(mixed[:, :, 0:head_rows].reshape(n_fs * rows, head_rows), w_o[shard, 0:head_rows, :])
@@ -781,10 +783,8 @@
         for k in range(2, n_sp - 1):
             head_part(arrivals[k][0])
 
-    for s, i in ((c_y, 1), (c_d, 0), (c_x, 1), (c_y, 0)):
-        arrive(conv_copy(s, i))
-    for s in others:
-        arrive(conv_relay(s, 0))
+    rest = (2 * n_fs - 1) * rows
+    arrive_all(w_o.at[0, pl.ds(0, rest), :], conv_recv.at[4])
 
     def place(core, shard):
         first = (shard % half_sp) * (n_fs * out_cols) + c * out_cols
@@ -794,7 +794,7 @@
         seq = others[j] if j < len(others) else c
         return remote(
             parts.at[shard, pl.ds(pl.multiple_of(seq * rows, LANES), rows), :], place(t, shard),
-            fin_recv.at[t, shard % half_sp, j], {"fs": seq, "tp": shard // half_sp},
+            fin_recv.at[t, shard % half_sp], {"fs": seq, "tp": shard // half_sp},
         )
 
     def keep_copy(shard):
@@ -815,23 +815,6 @@
         send(fin_copy(shard, len(others)), both(cond, jnp.logical_not(mine)))
         when(both(cond, mine), lambda: keep_copy(shard).start())
 
-    back_lanes = lanes_at(z % half_sp, n_fs * out_cols)
-    back_copy = remote(
-        part_o, placed.at[t, :, back_lanes], back_recv.at[t], {"sp": outer, "tp": z // half_sp}
-    )(back_send.at[0])
-    for name in ("hf", "cf"):
-        loads[name].wait()
-
-    def neighbour_part():
-        for i in (0, 1, *range(heads, heads + n_fs)):
-            arrive(to_near(i))
-        part_o[...] = dot(mixed_o[...], w_full[...]).astype(BF16)
-        back_copy.start()
-
-    @pl.when(inner)
-    def _():
-        neighbour_part()
-
     add_part(z)
     add_part(arrivals[0][0], inner)
     settle(C, 1)
@@ -846,6 +829,22 @@
         settle(C, k)
         add_part(arrivals[k][0])
 
+    back_lanes = lanes_at(z % half_sp, n_fs * out_cols)
+    back_copy = remote(
+        part_o, placed.at[t, :, back_lanes], back_recv.at[0], {"sp": outer, "tp": z // half_sp}
+    )(back_send.at[0])
+    for name in ("hf", "cf"):
+        loads[name].wait()
+
+    def neighbour_part():
+        arrive_all(mixed_o, up_recv.at[0])
+        part_o[...] = dot(mixed_o[...], w_full[...]).astype(BF16)
+        back_copy.start()
+
+    @pl.when(inner)
+    def _():
+        neighbour_part()
+
     for entry in sent[-RING:]:
         drain(entry)
 
@@ -859,27 +858,39 @@
         shard = t * half_sp + i
         computed = inner | (shard != near)
 
-        def arrived(core, j):
-            arrive(remote(parts.at[0, pl.ds(0, rows), :], place(0, i), fin_recv.at[core, i, j], {"tp": peer}))
-
         @pl.when(computed)
         def _():
-            for core in range(n_tp):
-                for j in range(len(others)):
-                    arrived(core, j)
-            arrived(peer, len(others))
+            arrive_all(parts.at[0, pl.ds(0, (n_fs - 1) * rows), :], fin_recv.at[t, i])
+            arrive_all(parts.at[0], fin_recv.at[peer, i])
             keep_copy(shard).wait()
 
         @pl.when(jnp.logical_not(computed))
         def _():
-            for core in range(n_tp):
-                arrive(remote(part_o, placed.at[0, :, lanes_at(i, n_fs * out_cols)], back_recv.at[core], {"tp": peer}))
+            arrive_all(parts.at[pl.ds(0, n_tp)], back_recv.at[0])
     log_copy.wait()
 
 
-def finish_kernel(placed, log_in, out, log_out):
-    out[...] = (placed[0].astype(F32) + placed[1].astype(F32)).astype(BF16)
-    log_out[...] = log_in[...]
+def finish_kernel(placed, log_in, out, log_out, held, summed, log_v, load_sem, store_sem):
+    span = out.shape[1] // 2
+    logs = pltpu.make_async_copy(log_in, log_v, load_sem.at[2])
+    loads = [
+        pltpu.make_async_copy(placed.at[:, :, pl.ds(i * span, span)], held.at[i], load_sem.at[i]) for i in range(2)
+    ]
+    for copy in loads:
+        copy.start()
+    logs.start()
+    stores = [
+        pltpu.make_async_copy(summed.at[i], out.at[:, pl.ds(i * span, span)], store_sem.at[i]) for i in range(2)
+    ]
+    for i in range(2):
+        loads[i].wait()
+        summed[i] = (held[i, 0].astype(F32) + held[i, 1].astype(F32)).astype(BF16)
+        stores[i].start()
+    logs.wait()
+    stores.append(pltpu.make_async_copy(log_v, log_out, store_sem.at[2]))
+    stores[2].start()
+    for copy in stores:
+        copy.wait()
 
 
 def fused_device(n_sp, n_fs, *args):
@@ -929,9 +940,9 @@
         pltpu.VMEM((rows, n_fs * out_cols), BF16),
         pltpu.VMEM((n_fs, halo, width), BF16),
         pltpu.VMEM((n_sp, n_fs * rows, out_cols), F32),
-        dma((10,)), dma((RING,)), dma((G + PIECES, n_sp - 1)), dma((2, n_sp - 1)), dma((2, 2)), dma((3,)), dma((n_fs,)),
-        dma((2, 2)), dma((2,)), dma((2,)), dma((n_fs, 2)), dma((2, half_sp, 4)), dma((1 + half_sp,)),
-        dma((2 + n_fs,)), dma((2,)), dma((1,)), dma((2,)), dma((2,)), dma((n_fs,)), dma((1,)), dma((2,)),
+        dma((10,)), dma((RING,)), dma((G + PIECES, n_sp - 1)), dma((2,)), dma((2, 2)), dma((1,)), dma((1,)),
+        dma((3,)), dma((2,)), dma((2,)), dma((5,)), dma((2, half_sp)), dma((1 + half_sp,)),
+        dma((1,)), dma((1,)), dma((1,)), dma((2,)), dma((1,)), dma((2,)),
     ]
     shapes = (
         jax.ShapeDtypeStruct((rows, half_sp * n_fs * out_cols), BF16),
@@ -948,7 +959,18 @@
         ),
         name="fused_layer",
     )(*operands)
-    return pl.pallas_call(finish_kernel, out_shape=shapes, name="finish")(placed, logs)
+    span = shapes[0].shape[1] // 2
+    return pl.pallas_call(
+        finish_kernel,
+        out_shape=shapes,
+        in_specs=[hbm] * 2,
+        out_specs=(hbm, hbm),
+        scratch_shapes=[
+            pltpu.VMEM((2, 2, rows, span), BF16), pltpu.VMEM((2, rows, span), BF16), pltpu.VMEM((heads, rows), F32),
+            dma((3,)), dma((3,)),
+        ],
+        name="finish",
+    )(placed, logs)
 
 
 def solution(mesh):

time: 48.7 us -> 49.6 us (1.018)
  Pallas kernels: 47.9 us -> 48.8 us
    pallas_call x1, Pallas kernels: 46.1 us -> 47 us  [fused_device(): pl.pallas_call(functools.partial(fused_kernel, n_sp), out_shape=(jax.Shap...]
where the time goes in v7:
time: 49.6 us; the launch traced here: 49.4 us
  Pallas kernels  48.8 us (98%)
  between operations  0.64 us (1%)
    pallas_call x1, Pallas kernels, fused_device(): pl.pallas_call(functools.partial(fused_kernel, n_sp), out_shape=(jax.Shap...  47 us
    pallas_call x1, Pallas kernels, fused_device(): pl.pallas_call(finish_kernel, out_shape=shapes, in_specs=[hbm] * 2, out_s...  1.77 us

profile of v7, /device:TPU:1, one launch (start us, length us, event | category | flops | bytes accessed | tf_op | source)
XLA Modules:
  0.0 49.4 jit_solution(9263958168965580065)
XLA Ops:
  0.6 47.0 %fused_layer.1 = (bf16[2,128,1024]{2,1,0:T(8,128)(2,1)}, f32[4,128]{1,0:T(4,128)}) custom-call(bf16[128,2048]{1,0:T(8,128)(2,1)} %tokens.1, bf16[2048]{0:T(1024)(128)(2,1)} %norm_gain_in.1, bf16[512,512]{1,0:T(8,128)(2,1)} %query_down.1, bf16[512]{0:T(512)(128)(2,1)} %query_gain_in.1, bf16[2048,256]{1,0:T(8,128)(2,1)} %latent_down.1, ...), custom_call_target="tpu_custom_call" | custom-call | tf_op jit(solution)/shard_map/fused_layer/pallas_call | solution.py:951
  47.7 1.8 %finish.1 = (bf16[128,1024]{1,0:T(8,128)(2,1)}, f32[4,128]{1,0:T(4,128)}) custom-call(bf16[2,128,1024]{2,1,0:T(8,128)(2,1)} %get-tuple-element.4.placed, f32[4,128]{1,0:T(4,128)} %get-tuple-element.5.log_in), custom_call_target="tpu_custom_call" | custom-call | tf_op jit(solution)/shard_map/finish/pallas_call | solution.py:963

commit v8 on v7

--- a/solution.py
+++ b/solution.py
@@ -182,7 +182,7 @@
 BF16 = jnp.bfloat16
 Q, K, H, C, G = range(5)
 PIECES = 4
-RING = 20
+RING = 28
 
 
 def rope_tables(length):

time: 49.6 us -> 48.4 us (0.976)
  Pallas kernels: 48.8 us -> 47.6 us
    pallas_call x1, Pallas kernels: 47 us -> 45.8 us  [fused_device(): pl.pallas_call(functools.partial(fused_kernel, n_sp), out_shape=(jax.Shap...]
where the time goes in v8:
time: 48.4 us; the launch traced here: 48.2 us
  Pallas kernels  47.6 us (98%)
  between operations  0.64 us (1%)
    pallas_call x1, Pallas kernels, fused_device(): pl.pallas_call(functools.partial(fused_kernel, n_sp), out_shape=(jax.Shap...  45.8 us
    pallas_call x1, Pallas kernels, fused_device(): pl.pallas_call(finish_kernel, out_shape=shapes, in_specs=[hbm] * 2, out_s...  1.77 us

profile of v8, /device:TPU:1, one launch (start us, length us, event | category | flops | bytes accessed | tf_op | source)
XLA Modules:
  0.0 48.2 jit_solution(18129194036242616566)
XLA Ops:
  0.6 45.8 %fused_layer.1 = (bf16[2,128,1024]{2,1,0:T(8,128)(2,1)}, f32[4,128]{1,0:T(4,128)}) custom-call(bf16[128,2048]{1,0:T(8,128)(2,1)} %tokens.1, bf16[2048]{0:T(1024)(128)(2,1)} %norm_gain_in.1, bf16[512,512]{1,0:T(8,128)(2,1)} %query_down.1, bf16[512]{0:T(512)(128)(2,1)} %query_gain_in.1, bf16[2048,256]{1,0:T(8,128)(2,1)} %latent_down.1, ...), custom_call_target="tpu_custom_call" | custom-call | tf_op jit(solution)/shard_map/fused_layer/pallas_call | solution.py:951
  46.5 1.8 %finish.1 = (bf16[128,1024]{1,0:T(8,128)(2,1)}, f32[4,128]{1,0:T(4,128)}) custom-call(bf16[2,128,1024]{2,1,0:T(8,128)(2,1)} %get-tuple-element.4.placed, f32[4,128]{1,0:T(4,128)} %get-tuple-element.5.log_in), custom_call_target="tpu_custom_call" | custom-call | tf_op jit(solution)/shard_map/finish/pallas_call | solution.py:963

commit v9 on v8

--- a/solution.py
+++ b/solution.py
@@ -674,8 +674,6 @@
         for k in range(1, last):
             add_arrival(k)
 
-    for h in range(2):
-        pass_head(h, at_end)
 
     @pl.when(at_end)
     def _():
@@ -752,10 +750,10 @@
     send(to_near(heads + c), at_end)
     for s, i, slot in ((c, 0, 1), (c_d, 1, 4), (c_y, 0, 4), (c, 1, 4), (c_d, 0, 4), (c_x, 1, 3)):
         send(conv_copy(s, i, slot))
+    pass_on(C, far, outer)
     pass_on(C, outer, far)
-    pass_on(C, far, outer)
     for h in range(2):
-        pass_head(h, inner)
+        pass_head(h, None)
     relay(H, last)
     arrive(conv_copy(c, 0, 0))
     send(to_near(heads + c_x), at_end)

time: 48.4 us -> 48.4 us (level)
  no operation moved by 1% of the time
where the time goes in v9:
time: 48.4 us; the launch traced here: 48.2 us
  Pallas kernels  47.6 us (98%)
  between operations  0.64 us (1%)
    pallas_call x1, Pallas kernels, fused_device(): pl.pallas_call(functools.partial(fused_kernel, n_sp), out_shape=(jax.Shap...  45.8 us
    pallas_call x1, Pallas kernels, fused_device(): pl.pallas_call(finish_kernel, out_shape=shapes, in_specs=[hbm] * 2, out_s...  1.77 us

profile of v9, /device:TPU:1, one launch (start us, length us, event | category | flops | bytes accessed | tf_op | source)
XLA Modules:
  0.0 48.2 jit_solution(5355858474633043826)
XLA Ops:
  0.6 45.8 %fused_layer.1 = (bf16[2,128,1024]{2,1,0:T(8,128)(2,1)}, f32[4,128]{1,0:T(4,128)}) custom-call(bf16[128,2048]{1,0:T(8,128)(2,1)} %tokens.1, bf16[2048]{0:T(1024)(128)(2,1)} %norm_gain_in.1, bf16[512,512]{1,0:T(8,128)(2,1)} %query_down.1, bf16[512]{0:T(512)(128)(2,1)} %query_gain_in.1, bf16[2048,256]{1,0:T(8,128)(2,1)} %latent_down.1, ...), custom_call_target="tpu_custom_call" | custom-call | tf_op jit(solution)/shard_map/fused_layer/pallas_call | solution.py:949
  46.5 1.8 %finish.1 = (bf16[128,1024]{1,0:T(8,128)(2,1)}, f32[4,128]{1,0:T(4,128)}) custom-call(bf16[2,128,1024]{2,1,0:T(8,128)(2,1)} %get-tuple-element.4.placed, f32[4,128]{1,0:T(4,128)} %get-tuple-element.5.log_in), custom_call_target="tpu_custom_call" | custom-call | tf_op jit(solution)/shard_map/finish/pallas_call | solution.py:961
